TPU v7x, 512 devices: a whole 4x8x8 slice. The times are simulated.
512 devices in a mesh: sp: 64 (over z, y), fs: 4 (over x), tp: 2 (over core).
Axes of the slice: x: 4, y: 8, z: 8, core: 2. Of those that a mesh axis runs over, the one named last changes fastest.
Arguments:
- tokens: bfloat16 [32768, 2048], P(('fs', 'sp')), may hold values from -6 to 6
- in_gain: float32 [2048], replicated, may hold values from 0.1 to 1.9
- query_weight: bfloat16 [2048, 512], P(None, ('tp', 'fs')), may hold values from -0.17291713 to 0.17291713
- key_weight: bfloat16 [2048, 512], P(None, ('tp', 'fs')), may hold values from -0.17291713 to 0.17291713
- value_weight: bfloat16 [2048, 512], P(None, ('tp', 'fs')), may hold values from -0.125 to 0.125
- rec_query_weight: bfloat16 [2048, 512], P(None, ('tp', 'fs')), may hold values from -0.125 to 0.125
- rec_forget_weight: bfloat16 [2048, 512], P(None, ('tp', 'fs')), may hold values from -0.125 to 0.125
- rec_input_weight: bfloat16 [2048, 512], P(None, ('tp', 'fs')), may hold values from -0.125 to 0.125
- mix_lambda: float32 [4], P('tp'), may hold values from 0.3 to 0.8
- lower_bound: float32 [4, 128], P('tp'), may hold values from 0.9 to 0.9999695
- forget_scale: float32 [32768], P(('fs', 'sp')), may hold values from 0.35 to 24576
- att_gain: float32 [128], replicated, may hold values from 0.1 to 1.9
- recurrence_gain: float32 [128], replicated, may hold values from 0.1 to 1.9
- att_out_weight: bfloat16 [512, 2048], P('tp'), may hold values from -0.1875 to 0.1875
- rec_out_weight: bfloat16 [512, 2048], P('tp'), may hold values from -0.1875 to 0.1875
Outputs:
- mixed_out: bfloat16 [32768, 2048], P(('fs', 'sp'))
- log_weight_sum: float32 [4, 32768], P('tp', ('fs', 'sp'))
All inputs are finite; a program needn't handle non-finite values.
Results may differ from a plain program's by a relative error of at most 0.012.
Values may be sent and summed in bfloat16 or wider, within the bound.
A program may use at most 128 MiB of HBM per device.

v0:
```python
import jax
import jax.numpy as jnp
from jax import lax
from jax.sharding import Mesh
from jax.sharding import PartitionSpec as P

DK = 64
DV = 128
BLK = 64
SP = ("sp_0", "sp_1")
FS_SP = ("fs", "sp_0", "sp_1")


EPS = 1e-06
NEG = -1e30


def in_one_piece(arrays, axis, dim, along):
    widths = [a.shape[along] for a in arrays]
    both = jnp.concatenate(arrays, axis=along)
    filled = lax.all_gather(both, axis, axis=dim, tiled=True)
    return tuple(jnp.split(filled, [sum(widths[:k]) for k in range(1, len(widths))], axis=along))


def nothing_yet(x, identity):
    return jax.tree.map(
        lambda part, zero: jnp.zeros_like(part) + jnp.asarray(zero, part.dtype), x, identity
    )


def entering(x, axes, combine, identity):
    before = start = nothing_yet(x, identity)
    running = x
    for axis in reversed(axes):
        peers, here = (lax.axis_size(axis), lax.axis_index(axis))
        pieces = jax.tree.map(lambda part: lax.all_gather(part, axis), running)
        inside, running = (start, start)
        for k in range(peers):
            passed = k < here
            running = combine(running, jax.tree.map(lambda part: part[k], pieces))
            inside = jax.tree.map(lambda new, old: jnp.where(passed, new, old), running, inside)
        before = combine(inside, before)
    return before


def copy_for_each(x, axis):
    peers = lax.axis_size(axis)
    return lax.all_to_all(jnp.broadcast_to(x[None], (peers, *x.shape)), axis, 0, 0, tiled=True)


def taken_together(x, axis):
    return copy_for_each(x, axis).astype(jnp.float32).sum(axis=0)


def norm_rows(values, gain):
    return values * lax.rsqrt(jnp.mean(values * values, axis=-1, keepdims=True) + EPS) * gain


def block_recurrence(queries, key_in, value_in, log_forget):
    head_count, row_count, key_width = queries.shape
    block_count = row_count // BLK

    def to_blocks(array_in):
        return array_in.reshape(head_count, block_count, BLK, array_in.shape[-1]).transpose(
            1, 0, 2, 3
        )

    causal = jnp.tril(jnp.ones((BLK, BLK), bool))

    def advance(passed_state, inputs):
        query_block, key_block, value_block, l_blk = inputs
        accumulator_sum = jnp.cumsum(l_blk, axis=1)
        cross_block_output = jnp.einsum(
            "sre,sei->sri",
            query_block * jnp.exp(accumulator_sum),
            passed_state,
            precision=lax.Precision.HIGHEST,
        )
        spread = accumulator_sum[:, :, None, :] - accumulator_sum[:, None, :, :]
        decay = jnp.exp(jnp.where(causal[None, :, :, None], spread, -jnp.inf))
        scores = jnp.einsum(
            "htk,htsk,hsk->hts", query_block, decay, key_block, precision=lax.Precision.HIGHEST
        )
        result = cross_block_output + jnp.einsum(
            "hts,hsv->htv", scores, value_block, precision=lax.Precision.HIGHEST
        )
        final_log_sum = accumulator_sum[:, -1:, :]
        updated_state = jnp.exp(final_log_sum[:, 0, :])[:, :, None] * passed_state + jnp.einsum(
            "plf,plt->pft",
            key_block * jnp.exp(final_log_sum - accumulator_sum),
            value_block,
            precision=lax.Precision.HIGHEST,
        )
        return (updated_state, result)

    begin_state = jnp.zeros((head_count, key_width, value_in.shape[-1]), jnp.float32)
    end_state, results = lax.scan(
        advance,
        begin_state,
        (to_blocks(queries), to_blocks(key_in), to_blocks(value_in), to_blocks(log_forget)),
    )
    return (
        end_state,
        results.transpose(1, 0, 2, 3).reshape(head_count, row_count, value_in.shape[-1]),
    )


def attend(online, queries, pair_keys, pair_values, allowed):
    running_max, weight_sum, numer_sum = online
    local_heads = numer_sum.shape[0]
    key_rows = pair_keys.shape[0]
    key_heads = pair_keys.reshape(key_rows, local_heads, 2, DK).transpose(1, 2, 0, 3)
    head_values = pair_values.reshape(key_rows, local_heads, DV).transpose(1, 0, 2)
    scores = jnp.einsum(
        "hmqd,hmkd->hmqk", queries, key_heads, preferred_element_type=jnp.float32
    ) * DK ** (-0.5)
    scores = jnp.where(allowed, scores, NEG)
    highest = jnp.maximum(running_max, jnp.max(scores, axis=-1))
    weights = jnp.exp(scores - highest[..., None])
    weight_sum = jnp.sum(weights, axis=-1)
    numer_sum = jnp.einsum(
        "itap,ipn->itan",
        weights.astype(jnp.bfloat16),
        head_values,
        preferred_element_type=jnp.float32,
    )
    return (highest, weight_sum, numer_sum)


def on_device(
    tokens,
    in_gain,
    query_weight,
    key_weight,
    value_weight,
    rec_query_weight,
    rec_forget_weight,
    rec_input_weight,
    mix_lambda,
    lower_bound,
    forget_scale,
    att_gain,
    recurrence_gain,
    att_out_weight,
    rec_out_weight,
):
    normed = norm_rows(tokens.astype(jnp.float32), in_gain).astype(jnp.bfloat16)
    row_count = normed.shape[0]
    stacked = jnp.stack(
        [
            query_weight,
            key_weight,
            value_weight,
            rec_query_weight,
            rec_forget_weight,
            rec_input_weight,
        ],
        axis=1,
    )
    projected = jnp.einsum(
        "rd,dnc->rnc",
        normed,
        lax.all_gather(stacked, "fs", axis=2, tiled=True),
        preferred_element_type=jnp.float32,
    ).astype(jnp.bfloat16)
    local_heads = projected.shape[2] // DV
    position = lax.axis_index(SP)
    query_pos = position * row_count + jnp.arange(row_count)
    queries = projected[:, 0].reshape(row_count, local_heads, 2, DK).transpose(1, 2, 0, 3)
    online = (
        jnp.full((local_heads, 2, row_count), NEG, jnp.float32),
        jnp.zeros((local_heads, 2, row_count), jnp.float32),
        jnp.zeros((local_heads, 2, row_count, DV), jnp.float32),
    )
    pair_keys, pair_values = in_one_piece((projected[:, 1], projected[:, 2]), SP, 0, 1)
    key_pos = jnp.arange(pair_keys.shape[0])
    allowed = query_pos[:, None] >= key_pos[None, :]
    online = lax.cond(
        jnp.int32(0) <= query_pos[-1],
        lambda state: attend(state, queries, pair_keys, pair_values, allowed),
        lambda state: state,
        online,
    )
    running_max, weight_sum, numer_sum = online
    mixed_heads = (
        numer_sum[:, 0] / weight_sum[:, 0, :, None]
        - mix_lambda[:, None, None] * numer_sum[:, 1] / weight_sum[:, 1, :, None]
    )
    att_heads = (norm_rows(mixed_heads, att_gain) * 0.8).astype(jnp.bfloat16)
    att_rows = att_heads.transpose(1, 0, 2).reshape(row_count, local_heads * DV)
    log_weight_sum = running_max[:, 0] + jnp.log(weight_sum[:, 0])

    def heads_first(array_in):
        return array_in.reshape(row_count, local_heads, DV).transpose(1, 0, 2).astype(jnp.float32)

    recurrent_queries = heads_first(projected[:, 3])
    lower_edge = lower_bound[:, None, :]
    forget = lower_edge + (1.0 - lower_edge) * jax.nn.sigmoid(heads_first(projected[:, 4]))
    log_forget = forget_scale[None, :, None] * jnp.log(forget)
    key_in = 1.0 - jnp.exp(log_forget)
    end_state, local_result = block_recurrence(
        recurrent_queries, key_in, heads_first(projected[:, 5]), log_forget
    )
    running_state = jnp.cumsum(log_forget, axis=1)
    carry_rate = jnp.exp(running_state[:, -1, :])

    def combine(earlier, later):
        return (later[0] * earlier[0], later[0][..., None] * earlier[1] + later[1])

    identity = (jnp.ones_like(carry_rate), jnp.zeros_like(end_state))
    _, incoming_state = entering((carry_rate, end_state), SP, combine, identity)
    combined = local_result + jnp.einsum(
        "zed,zdp->zep",
        recurrent_queries * jnp.exp(running_state),
        incoming_state,
        precision=lax.Precision.HIGHEST,
    )
    rec_heads = norm_rows(combined, recurrence_gain).astype(jnp.bfloat16)
    rec_rows = rec_heads.transpose(1, 0, 2).reshape(row_count, local_heads * DV)
    partial_value = jnp.dot(att_rows, att_out_weight, preferred_element_type=jnp.float32) + jnp.dot(
        rec_rows, rec_out_weight, preferred_element_type=jnp.float32
    )
    mixed_out = (
        taken_together(partial_value.astype(jnp.bfloat16), "tp")
        .astype(jnp.float32)
        .astype(jnp.bfloat16)
    )
    return (mixed_out, log_weight_sum)


def solution(mesh):
    finer = Mesh(
        mesh.devices.reshape(8, 8, mesh.shape["fs"], mesh.shape["tp"]), ("sp_0", "sp_1", "fs", "tp")
    )
    placed = (
        P(FS_SP, None),
        P(),
        P(None, ("tp", "fs")),
        P(None, ("tp", "fs")),
        P(None, ("tp", "fs")),
        P(None, ("tp", "fs")),
        P(None, ("tp", "fs")),
        P(None, ("tp", "fs")),
        P("tp"),
        P("tp", None),
        P(FS_SP),
        P(),
        P(),
        P("tp", None),
        P("tp", None),
    )
    return jax.shard_map(
        on_device,
        mesh=finer,
        in_specs=placed,
        out_specs=(P(FS_SP, None), P("tp", FS_SP)),
        check_vma=False,
    )
```

profile of v0, /device:TPU:1, one launch (start us, length us, event | category | flops | bytes accessed | tf_op | source)
XLA Modules:
  0.0 367.2 jit_solution(1742700413866512903)
XLA Ops:
  7.3 1.1 bitcast_dynamic-update-slice_fusion.5
  8.3 1.0 bitcast_dynamic-update-slice_fusion.4
  9.3 1.0 bitcast_dynamic-update-slice_fusion.3
  10.3 1.0 bitcast_dynamic-update-slice_fusion.2
  11.3 1.0 bitcast_dynamic-update-slice_fusion.1
  12.2 1.0 bitcast_dynamic-update-slice_fusion
  13.2 1.1 copy-done.2
  14.5 0.2 fusion.42
  14.7 76.1 %all-gather.7.cloned.1.call-done = bf16[2048,6,256]{0,2,1:T(8,128)(2,1)} async-done(((bf16[2048,6,64]{0,2,1:T(8,128)(2,1)}), bf16[2048,6,256]{0,2,1:T(8,128)(2,1)}) %all-gather.7.cloned.1.call-update) | async-done | bytes 6291472 | tf_op jit(solution)/shard_map/all_gather | solution.py:163
  90.8 5.0 %convolution_convert_fusion = bf16[128,6,256]{2,0,1:T(8,128)(2,1)S(1)} fusion(bf16[2048,6,256]{0,2,1:T(8,128)(2,1)} %all-gather.7.cloned.1.call-done, bf16[128,2048]{1,0:T(8,128)(2,1)S(1)} %copy-done.3, f32[2048]{0:T(1024)S(1)} %copy-done.5, f32[128]{0:T(128)S(1)} %add_rsqrt_fusion.2), kind=kOutput, calls=%fused_computation.55 | convolution fusion | flops 806551552 | bytes 7217664 | tf_op jit(solution)/shard_map/rd,dnc->rnc/dot_general | solution.py:160
  96.3 16.1 %while.13 = (s32[]{:T(128)}, f32[2,128,128]{2,1,0:T(8,128)S(1)}, f32[2,2,64,128]{3,2,0,1:T(8,128)S(1)}, f32[2,2,64,128]{3,2,0,1:T(8,128)S(1)}, f32[2,2,64,128]{3...) while((s32[]{:T(128)}, f32[2,128,128]{2,1,0:T(8,128)S(1)}, ...), condition=%wide.region_8.9_spmd.clone, body=%wide.region_6.8_spmd.clone.sunk | while | flops 79876096 | bytes 1819267 | solution.py:97
  96.5 6.9 %fusion.202 = f32[2,64,1,64]{3,2,1,0:T(1,128)S(1)} fusion(f32[2,64,128,1]{2,3,1,0:T(1,128)S(1)} %bitcast.358, f32[2,64,128]{2,1,0:T(8,128)S(1)} %get-tuple-element.238, f32[2,64,128]{2,1,0:T(8,128)S(1)} %reduce_window_sum.25, pred[64,64]{1,0:T(8,128)(4,1)S(1)} %iota_compare_fusion.2), kind=kOutput, calls=%fused_computation.14.clone.1 | convolution fusion | flops 15728640 | bytes 233472 | tf_op jit(solution)/shard_map/while/body/eval_jaxpr/htk,htsk,hsk->hts/dot_general | solution.py:81
  103.4 0.3 fusion.201
  103.7 0.2 fusion.203
  103.9 0.4 convolution_add_fusion.5
  104.5 6.9 %fusion.202 = f32[2,64,1,64]{3,2,1,0:T(1,128)S(1)} fusion(f32[2,64,128,1]{2,3,1,0:T(1,128)S(1)} %bitcast.358, f32[2,64,128]{2,1,0:T(8,128)S(1)} %get-tuple-element.238, f32[2,64,128]{2,1,0:T(8,128)S(1)} %reduce_window_sum.25, pred[64,64]{1,0:T(8,128)(4,1)S(1)} %iota_compare_fusion.2), kind=kOutput, calls=%fused_computation.14.clone.1 | convolution fusion | flops 15728640 | bytes 233472 | tf_op jit(solution)/shard_map/while/body/eval_jaxpr/htk,htsk,hsk->hts/dot_general | solution.py:81
  111.4 0.3 fusion.201
  111.7 0.2 fusion.203
  111.9 0.4 convolution_add_fusion.5
  112.4 0.6 copy-done.1
  113.1 0.2 reduce_window_sum.22
  113.3 12.4 %all-gather = f32[16,1,128]{2,1,0:T(1,128)S(1)} all-gather(f32[2,1,128]{2,1,0:T(1,128)S(1)} %slice_exponential_fusion), channel_id=2, replica_groups=mesh['sp_0'=8,'sp_1'=8,'fs'=4,'tp'=2] {'sp_1'}, dimensions={0}, use_global_device_ids=true | all-gather | bytes 9216 | tf_op jit(solution)/shard_map/all_gather | solution.py:36
  125.7 24.3 %all-gather.13.cloned.1.call-done = f32[16,128,128]{2,1,0:T(8,128)} async-done(((f32[2,128,128]{2,1,0:T(8,128)}), f32[16,128,128]{2,1,0:T(8,128)}) %all-gather.13.cloned.1.call-update) | async-done | bytes 1048592 | tf_op jit(solution)/shard_map/all_gather | solution.py:36
  150.0 2.3 bitcast_add_fusion
  152.4 0.7 pad_maximum_fusion
  153.1 0.6 slice.141
  154.2 0.1 copy.85
  154.4 13.5 %all_gather.27 = f32[8,2,128]{2,1,0:T(2,128)S(1)} all-gather(f32[1,2,128]{2,1,0:T(2,128)S(1)} %get-tuple-element.183), channel_id=1, replica_groups=mesh['sp_0'=8,'sp_1'=8,'fs'=4,'tp'=2] {'sp_0'}, dimensions={0}, use_global_device_ids=true | all-gather | bytes 9216 | tf_op jit(solution)/shard_map/all_gather | solution.py:36
  168.0 25.6 %all-gather.11.cloned.1.call-done = f32[8,2,128,128]{3,2,1,0:T(8,128)} async-done(((f32[1,2,128,128]{3,2,1,0:T(8,128)}), f32[8,2,128,128]{3,2,1,0:T(8,128)}) %all-gather.11.cloned.1.call-update) | async-done | bytes 1048592 | tf_op jit(solution)/shard_map/all_gather | solution.py:36
  193.5 2.6 multiply_reduce_fusion
  196.3 102.3 %all-gather.9.cloned.1.call-done = bf16[8192,512]{1,0:T(8,128)(2,1)} async-done(((bf16[128,512]{1,0:T(8,128)(2,1)}), bf16[8192,512]{1,0:T(8,128)(2,1)}) %all-gather.9.cloned.1.call-update) | async-done | bytes 8388624 | tf_op jit(solution)/shard_map/all_gather | solution.py:21
  298.6 0.4 ge.22
  299.0 53.7 %conditional.1 = (f32[2,2,128]{2,1,0:T(2,128)S(1)}, f32[2,2,128,128]{3,2,1,0:T(8,128)S(1)}, f32[2,128]{1,0:T(2,128)S(1)}) conditional(s32[]{:T(128)} %bitcast.8, () %tuple.22, (s32[]{:T(128)}, s32[128,1]{0,1:T(1,128)S(1)}, s32[128,8192]{1,0:T(8,128)S(1)}, bf16[8192,512]{1,0:T(8,128)(2,1)}, bf16[2,2,128,64]{2,3,1,0:T(8,128)(2,1)S(1)}) %tuple.88), branch_computations={%region_1.0_spmd, %region_2.5_spmd} | conditional | flops 1657798272 | bytes 109395480 | solution.py:178
  299.2 0.7 broadcast_compare_fusion
  299.9 11.9 %copy.86 = bf16[8192,512]{0,1:T(8,128)(2,1)} copy(bf16[8192,512]{1,0:T(8,128)(2,1)} %get-tuple-element.135) | data formatting | bytes 16777216 | tf_op jit(solution)/shard_map
  311.8 5.9 %fusion.173 = (bf16[8192,256]{0,1:T(8,128)(2,1)}, bf16[8192,256]{0,1:T(8,128)(2,1)}) fusion(bf16[8192,512]{0,1:T(8,128)(2,1)} %copy.86), kind=kLoop, calls=%fused_computation.242 | loop fusion | bytes 16777216 | tf_op jit(solution)/shard_map/split | solution.py:22
  317.8 6.3 %copy.84 = bf16[8192,2,128]{2,0,1:T(8,128)(2,1)} copy(bf16[8192,2,128]{0,2,1:T(8,128)(2,1)} %bitcast.357) | data formatting | bytes 8388608 | tf_op jit(solution)/shard_map/cond/branch_1_fun/reshape | solution.py:113
  324.1 11.2 %fusion.2 = (f32[2,2,128]{2,1,0:T(2,128)S(1)}, f32[2,2,128,8192]{3,2,1,0:T(8,128)}) fusion(pred[128,8192]{1,0:T(8,128)(4,1)S(1)} %broadcast_compare_fusion, bf16[2,2,128,64]{2,3,1,0:T(8,128)(2,1)S(1)} %get-tuple-element.54, bf16[2,2,8192,64]{2,3,1,0:T(8,128)(2,1)} %bitcast.361), kind=kOutput, calls=%fused_computation.3 | convolution fusion | flops 549453312 | bytes 22087680 | tf_op jit(solution)/shard_map/cond/branch_1_fun/hmqd,hmkd->hmqk/dot_general | solution.py:114
  335.3 9.3 %fusion.5 = f32[2,2,128,128]{3,2,1,0:T(8,128)S(1)} fusion(f32[2,2,128,8192]{3,2,1,0:T(8,128)} %get-tuple-element.165, f32[2,2,128]{2,1,0:T(2,128)S(1)} %broadcast_maximum_fusion, pred[128,8192]{1,0:T(8,128)(4,1)S(1)} %broadcast_compare_fusion, bf16[8192,2,128]{2,0,1:T(8,128)(2,1)} %copy.84), kind=kOutput, calls=%fused_computation.6 | convolution fusion | flops 1090519040 | bytes 22284288 | tf_op jit(solution)/shard_map/cond/branch_1_fun/itap,ipn->itan/dot_general | solution.py:121
  344.6 8.1 %fusion.4 = f32[2,2,128]{2,1,0:T(2,128)S(1)} fusion(f32[2,2,128,8192]{3,2,1,0:T(8,128)} %get-tuple-element.165, f32[2,2,128]{2,1,0:T(2,128)S(1)} %broadcast_maximum_fusion, pred[128,8192]{1,0:T(8,128)(4,1)S(1)} %broadcast_compare_fusion), kind=kLoop, calls=%fused_computation.5 | loop fusion | flops 16776704 | bytes 17829888 | tf_op jit(solution)/shard_map/cond/branch_1_fun/reduce_sum | solution.py:120
  352.7 0.1 copy.87
  352.9 0.6 log_add_fusion
  353.4 0.1 multiply_reduce_fusion.1
  353.7 0.3 fusion.174
  354.0 0.3 fusion.41
  354.3 0.1 broadcast_in_dim.46
  354.5 5.1 %all_to_all.5 = bf16[2,128,2048]{2,1,0:T(8,128)(2,1)S(1)} all-to-all(bf16[2,128,2048]{2,1,0:T(8,128)(2,1)S(1)} %broadcast_in_dim.46), channel_id=1, replica_groups=mesh['sp_0'=8,'sp_1'=8,'fs'=4,'tp'=2] {'tp'}, dimensions={0} | all-to-all | bytes 2097152 | tf_op jit(solution)/shard_map/all_to_all | solution.py:48
  359.6 1.1 reduce_sum.51
  (71 shorter events, 1.4 us)
Async XLA Ops:
  7.2 346.5 %copy-start = (bf16[256,2048]{1,0:T(8,128)(2,1)S(1)}, bf16[256,2048]{1,0:T(8,128)(2,1)}, u32[]{:S(2)}) copy-start(bf16[256,2048]{1,0:T(8,128)(2,1)} %param.32) | copy-start | bytes 3145732
  7.2 7.3 %copy-start.3 = (bf16[128,2048]{1,0:T(8,128)(2,1)S(1)}, bf16[128,2048]{1,0:T(8,128)(2,1)}, u32[]{:S(2)}) copy-start(bf16[128,2048]{1,0:T(8,128)(2,1)} %param.19) | copy-start | bytes 1572868
  7.2 7.5 %copy-start.6 = (f32[2,128]{1,0:T(2,128)S(1)}, f32[2,128]{1,0:T(2,128)}, u32[]{:S(2)}) copy-start(f32[2,128]{1,0:T(2,128)} %param.28) | copy-start | bytes 3076
  7.2 83.6 %copy-start.5 = (f32[2048]{0:T(1024)S(1)}, f32[2048]{0:T(1024)}, u32[]{:S(2)}) copy-start(f32[2048]{0:T(1024)} %param.20) | copy-start | bytes 24580
  7.2 83.6 %all-gather.7.cloned.1.call-start = ((), (), s32[]{:S(2)}) async-start(), calls=%async_computation.1 | async-start | bytes 7864320 | tf_op jit(solution)/shard_map/all_gather | solution.py:163
  13.2 1.1 copy-start.2
  14.4 135.6 %all-gather.13.cloned.1.call-start = ((), (), s32[]{:S(2)}) async-start(), calls=%async_computation.4 | async-start | bytes 1179648 | tf_op jit(solution)/shard_map/all_gather | solution.py:36
  14.7 81.5 %copy-start.7 = (f32[128]{0:T(128)S(1)}, f32[128]{0:T(128)}, u32[]{:S(2)}) copy-start(f32[128]{0:T(128)} %param.29) | copy-start | bytes 1540
  112.4 0.7 copy-start.1
  112.4 83.8 %copy-start.8 = (f32[128]{0:T(128)S(1)}, f32[128]{0:T(128)}, u32[]{:S(2)}) copy-start(f32[128]{0:T(128)} %param.31) | copy-start | bytes 1540
  113.0 80.5 %all-gather.11.cloned.1.call-start = ((), (), s32[]{:S(2)}) async-start(), calls=%async_computation.3 | async-start | bytes 1179648 | tf_op jit(solution)/shard_map/all_gather | solution.py:36
  152.3 146.3 %all-gather.9.cloned.1.call-start = ((), (), s32[]{:S(2)}) async-start(), calls=%async_computation.2 | async-start | bytes 8519680 | tf_op jit(solution)/shard_map/all_gather | solution.py:21
  299.0 54.5 %copy-start.9 = (f32[2]{0:T(128)S(1)}, f32[2]{0:T(128)}, u32[]{:S(2)}) copy-start(f32[2]{0:T(128)} %param.27) | copy-start | bytes 28
  299.0 54.6 %copy-start.10 = (f32[128]{0:T(128)S(1)}, f32[128]{0:T(128)}, u32[]{:S(2)}) copy-start(f32[128]{0:T(128)} %param.30) | copy-start | bytes 1540
  299.0 55.0 %copy-start.4 = (bf16[256,2048]{1,0:T(8,128)(2,1)S(1)}, bf16[256,2048]{1,0:T(8,128)(2,1)}, u32[]{:S(2)}) copy-start(bf16[256,2048]{1,0:T(8,128)(2,1)} %param.33) | copy-start | bytes 3145732
Sparse Core Ops, SparseCore 0:
  14.5 76.2 all-gather.6
  113.2 36.8 all-gather.12
  152.4 41.0 all-gather.10
  197.0 101.4 all-gather.8
where the time goes:
time: 368 us; the launch traced here: 367 us
  waiting for transfers between devices  228 us (62%)
  matrix products  44.4 us (12%)
  local copies, waits for them, and re-layouts  33.7 us (9%)
  blocking collectives  31 us (8%)
  between operations  14.8 us (4%)
  other arithmetic  14.5 us (4%)
    all_gather x1, waiting for transfers between devices, in_one_piece(): filled = lax.all_gather(both, axis, axis=dim, tiled=True)  102 us
    all_gather x1, waiting for transfers between devices, on_device(): lax.all_gather(stacked, 'fs', axis=2, tiled=True)  76.1 us
    all_gather x2, waiting for transfers between devices, entering(): pieces = jax.tree.map(lambda part: lax.all_gather(part, axis), running)  49.9 us
    all_gather x2, blocking collectives, entering(): pieces = jax.tree.map(lambda part: lax.all_gather(part, axis), running)  25.9 us
    dot_general x2, matrix products, advance(): jnp.einsum('htk,htsk,hsk->hts', query_block, decay, key_block, precision=...  13.9 us
    another operation x1, local copies, waits for them, and re-layouts  11.9 us
    dot_general x1, matrix products, attend(): jnp.einsum('hmqd,hmkd->hmqk', queries, key_heads, preferred_element_type=...  11.2 us
    dot_general x1, matrix products, attend(): jnp.einsum('itap,ipn->itan', weights.astype(jnp.bfloat16), head_values, p...  9.28 us
  transfers between devices with their start and end apart: 4, of which 4 were waited for; matrix products, arithmetic and copies ran while one was open for 1% of the time, Pallas kernels for 0%

commit v1 on v0

v1 whole, which is shorter than its diff:
```python
import functools

import jax
import jax.numpy as jnp
from jax import lax
from jax.experimental import pallas as pl
from jax.experimental.pallas import tpu as pltpu
from jax.sharding import PartitionSpec as P

DK = 64
DV = 128
ROWS = 128
COLS = 384
EPS = 1e-06
NEG = -1e30
FS = 4
PARTS = 4
MESH = pl.DeviceIdType.MESH
F32 = jnp.float32
BF16 = jnp.bfloat16


def dot_nn(a, b):
    return lax.dot_general(a, b, (((1,), (0,)), ((), ())), preferred_element_type=F32)


def dot_nt(a, b):
    return lax.dot_general(a, b, (((1,), (1,)), ((), ())), preferred_element_type=F32)


def norm_rows(values, gain):
    mean = jnp.mean(values * values, axis=-1, keepdims=True)
    return values * lax.rsqrt(mean + EPS) * gain


def kernel_body(
    nz, ny,
    tok_hbm, gain_ref, wq, wk, wv, wrq, wrf, wri, lam_ref, lb_ref, scale_ref, attg_ref, recg_ref,
    wa_hbm, wr_hbm,
    out_ref, lws_ref,
    tok, wraw, wcat, wo, nrm, res, rsend,
    gy, gz, s_scr, e_scr,
    o0s, o0r, t0s, t0r, o1s, o1r, t1s, t1r,
    st_s, st_r, tot_s, tot_r, in_s, in_r, pref, qc_scr, ol_scr,
    pbuf, prx,
    lsem, a_send, a_recv, r_send, r_recv,
    gy_send, gy_recv, gz_send, gz_recv,
    o0_send, o0_recv, t0_send, t0_recv, o1_send, o1_recv, t1_send, t1_recv,
    st_send, st_recv, tot_send, tot_recv, in_send, in_recv,
    p_send, p_recv,
):
    p = lax.axis_index("sp")
    x = lax.axis_index("fs")
    t = lax.axis_index("tp")
    z = p // ny
    y = p % ny
    t_other = 1 - t
    xl = (x + 3) % 4
    xr = (x + 1) % 4
    xo = (x + 2) % 4
    slice_rows = DV // ny

    weights = (wq, wk, wv, wrq, wrf, wri)
    tok_copy = pltpu.make_async_copy(tok_hbm, tok, lsem.at[0])
    tok_copy.start()
    w_copies = [pltpu.make_async_copy(w, wraw.at[i], lsem.at[1 + i]) for i, w in enumerate(weights)]
    for c in w_copies:
        c.start()
    wo_copies = [
        pltpu.make_async_copy(wa_hbm, wo.at[0], lsem.at[7]),
        pltpu.make_async_copy(wr_hbm, wo.at[1], lsem.at[8]),
    ]
    for c in wo_copies:
        c.start()

    barrier = pltpu.get_barrier_semaphore()

    def greet(dev):
        pl.semaphore_signal(barrier, inc=1, device_id=dev, device_id_type=MESH)

    greet({"tp": t_other})
    for d in range(1, 4):
        greet({"fs": (x + d) % 4})
    for d in range(1, ny):
        greet({"sp": z * ny + (y + d) % ny})
    for d in range(1, nz):
        greet({"sp": ((z + d) % nz) * ny + y})

    def remote(src, dst, ssem, rsem, dev):
        return pltpu.make_async_remote_copy(
            src_ref=src, dst_ref=dst, send_sem=ssem, recv_sem=rsem, device_id=dev, device_id_type=MESH
        )

    def piece(f, tt, pc):
        return nrm.at[f, pl.ds(pl.multiple_of(tt * 64 + pc * 32, 32), 32)]

    def a_sem(f, tt, pc):
        return a_recv.at[f, tt * 2 + pc]

    def normalise(tt, pc):
        rows = pl.ds(pl.multiple_of(tt * 64 + pc * 32, 32), 32)
        nrm[x, rows, :] = norm_rows(tok[rows, :].astype(F32), gain_ref[...]).astype(BF16)

    tok_copy.wait()
    normalise(t, 0)
    normalise(t, 1)
    pl.semaphore_wait(barrier, 1 + 3 + (ny - 1) + (nz - 1))

    a_list = []

    def a_start(k, f, pc, dev):
        c = remote(piece(f, t, pc), piece(f, t, pc), a_send.at[k], a_sem(f, t, pc), dev)
        c.start()
        a_list.append(c)

    def a_wait(f, tt, pc):
        remote(piece(f, tt, pc), piece(f, tt, pc), a_send.at[0], a_sem(f, tt, pc), {"fs": xr}).wait_recv()

    a_start(0, x, 0, {"fs": xr})
    a_start(1, x, 1, {"fs": xl})
    a_start(2, x, 1, {"fs": xr})
    a_start(3, x, 0, {"fs": xl})
    normalise(t_other, 0)
    normalise(t_other, 1)
    for i in range(6):
        w_copies[i].wait()
        wcat[:, i * 64:(i + 1) * 64] = wraw[i]

    def project(f):
        return dot_nn(nrm[f], wcat[...]).astype(BF16)

    res[x] = project(x)
    a_wait(xl, t, 0)
    a_start(4, xl, 0, {"fs": xr})
    a_start(5, xl, 0, {"tp": t_other})
    a_wait(xr, t, 1)
    a_start(6, xr, 1, {"fs": xl})
    a_start(7, xr, 1, {"tp": t_other})
    a_wait(xl, t, 1)
    a_start(8, xl, 1, {"tp": t_other})
    a_wait(xr, t, 0)
    a_start(9, xr, 0, {"tp": t_other})

    r_list = []

    def answer(k, f):
        a_wait(f, t_other, 0)
        a_wait(f, t_other, 1)
        rsend[k] = project(f)
        c = remote(rsend.at[k], res.at[x], r_send.at[k], r_recv.at[x], {"fs": f})
        c.start()
        r_list.append(c)

    answer(0, xl)
    answer(1, xr)
    a_wait(xo, t, 0)
    a_start(10, xo, 0, {"tp": t_other})
    a_wait(xo, t, 1)
    a_start(11, xo, 1, {"tp": t_other})
    answer(2, xo)
    for f in (xl, xr, xo):
        remote(res.at[f], res.at[f], r_send.at[0], r_recv.at[f], {"fs": xr}).wait_recv()

    def tile(kind, h):
        lo = kind * 64
        return jnp.concatenate([res[2 * h, :, lo:lo + 64], res[2 * h + 1, :, lo:lo + 64]], axis=1)

    def value_t(h):
        return tile(2, h).astype(F32).T.astype(BF16)

    scale_q = jnp.asarray(DK ** (-0.5), BF16)
    gy[y, 0] = tile(0, 0) * scale_q
    gy[y, 1] = tile(1, 1)
    gy[y, 2] = value_t(1)
    gz[z, 0] = tile(0, 1) * scale_q
    gz[z, 1] = tile(1, 0)
    gz[z, 2] = value_t(0)

    def y_dev(yy):
        return {"sp": z * ny + yy}

    def z_dev(zz):
        return {"sp": zz * ny + y}

    g_list = []
    for d in range(1, max(ny, nz)):
        if d < ny:
            c = remote(gy.at[y], gy.at[y], gy_send.at[d], gy_recv.at[y], y_dev((y + d) % ny))
            c.start()
            g_list.append(c)
        if d < nz:
            c = remote(gz.at[z], gz.at[z], gz_send.at[d], gz_recv.at[z], z_dev((z + d) % nz))
            c.start()
            g_list.append(c)

    row = lax.broadcasted_iota(jnp.int32, (ROWS, ROWS), 0)
    col = lax.broadcasted_iota(jnp.int32, (ROWS, ROWS), 1)
    tril = jnp.where(row >= col, 1.0, 0.0).astype(F32)
    scale_col = jnp.broadcast_to(scale_ref[...], (ROWS, ROWS)).T
    for h in range(2):
        rq = tile(3, h).astype(F32)
        rf = tile(4, h).astype(F32)
        ri = tile(5, h)
        edge = lb_ref[h:h + 1, :]
        forget = edge + (1.0 - edge) * jax.nn.sigmoid(rf)
        g = scale_col * jnp.log(forget)
        kk = 1.0 - jnp.exp(g)
        cum = lax.dot_general(
            tril, g, (((1,), (0,)), ((), ())), precision=lax.Precision.HIGHEST, preferred_element_type=F32
        )
        scores = jnp.where(row == col, jnp.sum(rq * kk, axis=-1, keepdims=True), 0.0)
        c8 = cum.reshape(ROWS // 8, 8, DV)
        r8 = lax.broadcasted_iota(jnp.int32, (ROWS // 8, 8, DV), 1)
        for b in (64, 32, 16, 8, 4, 2, 1):
            if b >= 8:
                c3 = cum.reshape(ROWS // (2 * b), 2 * b, DV)
                diff = (c3 - c3[:, b - 1:b, :]).reshape(ROWS, DV)
            else:
                mid = c8[:, b - 1:b, :]
                for first in range(2 * b, 8, 2 * b):
                    mid = jnp.where(r8 >= first, c8[:, first + b - 1:first + b, :], mid)
                diff = (c8 - mid).reshape(ROWS, DV)
            upper = (row & (2 * b - 1)) >= b
            decay = jnp.exp(jnp.where(upper, diff, -diff))
            late = jnp.where(upper, rq * decay, 0.0).astype(BF16)
            early = jnp.where(upper, 0.0, kk * decay).astype(BF16)
            level = dot_nt(late, early)
            scores = scores + jnp.where((row ^ col) < 2 * b, level, 0.0)
        ol_scr[h] = dot_nn(scores.astype(BF16), ri)
        last = cum[ROWS - 1:ROWS, :]
        key_end = (kk * jnp.exp(last - cum)).astype(BF16)
        state_t = dot_nn(ri.astype(F32).T.astype(BF16), key_end)
        qc_scr[h] = (rq * jnp.exp(cum)).astype(BF16)
        st_s[:, h * slice_rows:(h + 1) * slice_rows, :] = state_t.reshape(ny, slice_rows, DV)
        st_s[:, 2 * slice_rows + 8 * h:2 * slice_rows + 8 * h + 8, :] = jnp.broadcast_to(
            jnp.exp(last).reshape(1, 1, DV), (ny, 8, DV)
        )
    st_r[y] = st_s[y]
    for d in range(1, ny):
        yy = (y + d) % ny
        c = remote(st_s.at[yy], st_r.at[y], st_send.at[d], st_recv.at[y], y_dev(yy))
        c.start()
        g_list.append(c)

    for d in range(1, ny):
        yy = (y + d) % ny
        remote(st_r.at[yy], st_r.at[yy], st_send.at[0], st_recv.at[yy], y_dev(yy)).wait_recv()
    half = slice_rows
    for h in range(2):
        state = jnp.zeros((half, DV), F32)
        rate = jnp.ones((8, DV), F32)
        for k in range(ny):
            pref[k, h * half:(h + 1) * half, :] = state
            pref[k, 2 * half + 8 * h:2 * half + 8 * h + 8, :] = rate
            step = st_r[k, 2 * half + 8 * h:2 * half + 8 * h + 8, :]
            state = step[0:1, :] * state + st_r[k, h * half:(h + 1) * half, :]
            rate = rate * step
        tot_s[h * half:(h + 1) * half, :] = state
        tot_s[2 * half + 8 * h:2 * half + 8 * h + 8, :] = rate
    for d in range(1, nz):
        zz = (z + d) % nz
        c = remote(tot_s, tot_r.at[z], tot_send.at[d], tot_recv.at[z], z_dev(zz))
        c.start()
        g_list.append(c)

    for d in range(1, nz):
        zz = (z + d) % nz
        remote(tot_r.at[zz], tot_r.at[zz], tot_send.at[0], tot_recv.at[zz], z_dev(zz)).wait_recv()

    def fold(k, carry):
        s0, s1 = carry
        d0 = tot_r[k, 2 * half:2 * half + 1, :]
        d1 = tot_r[k, 2 * half + 8:2 * half + 9, :]
        return (d0 * s0 + tot_r[k, 0:half, :], d1 * s1 + tot_r[k, half:2 * half, :])

    entry = lax.fori_loop(0, z, fold, (jnp.zeros((half, DV), F32), jnp.zeros((half, DV), F32)))
    for k in range(ny):
        for h in range(2):
            d = pref[k, 2 * half + 8 * h:2 * half + 8 * h + 1, :]
            in_s[k, h] = (d * entry[h] + pref[k, h * half:(h + 1) * half, :]).astype(BF16)
    in_r[y] = in_s[y]
    for d in range(1, ny):
        yy = (y + d) % ny
        c = remote(in_s.at[yy], in_r.at[y], in_send.at[d], in_recv.at[y], y_dev(yy))
        c.start()
        g_list.append(c)

    for d in range(1, ny):
        yy = (y + d) % ny
        remote(gy.at[yy], gy.at[yy], gy_send.at[0], gy_recv.at[yy], y_dev(yy)).wait_recv()
    for d in range(1, nz):
        zz = (z + d) % nz
        remote(gz.at[zz], gz.at[zz], gz_send.at[0], gz_recv.at[zz], z_dev(zz)).wait_recv()

    lane = lax.broadcasted_iota(jnp.int32, (ROWS, DV), 1)

    def unit(queries, tiles, count, limits, masked_from, o_out, t_out):
        zero = jnp.zeros_like(queries)
        both = jnp.concatenate(
            [jnp.where(lane < DK, queries, zero), jnp.where(lane < DK, zero, queries)], axis=0
        )
        top = jnp.full((8, 2 * ROWS), NEG, F32)
        for k in range(count):
            s = dot_nt(tiles[k, 1], both)
            if k >= masked_from:
                ri_ = lax.broadcasted_iota(jnp.int32, (ROWS, 2 * ROWS), 0)
                ci_ = lax.broadcasted_iota(jnp.int32, (ROWS, 2 * ROWS), 1) & (ROWS - 1)
                s = jnp.where(ri_ - ci_ <= limits(k), s, NEG)
            s_scr[k] = s
            top = jnp.maximum(top, jnp.max(s.reshape(ROWS // 8, 8, 2 * ROWS), axis=0))
        top = jnp.max(top, axis=0, keepdims=True)
        total = jnp.zeros((8, 2 * ROWS), F32)
        num = jnp.zeros((DV, 2 * ROWS), F32)
        for k in range(count):
            e = jnp.exp(s_scr[k] - top)
            total = total + jnp.sum(e.reshape(ROWS // 8, 8, 2 * ROWS), axis=0)
            num = num + dot_nn(tiles[k, 2], e.astype(BF16))
        total = jnp.sum(total, axis=0, keepdims=True)
        o_out[...] = num.astype(BF16)
        t_out[0:1, :] = top
        t_out[1:2, :] = total

    def head0(count):
        def body(yq, carry):
            unit(
                gy[yq, 0], gz, count,
                lambda k: ((z - k) * ny + (yq - y)) * ROWS,
                count - 2, o0s.at[yq], t0s.at[yq],
            )

            @pl.when(yq != y)
            def _():
                remote(o0s.at[yq], o0r.at[y], o0_send.at[yq], o0_recv.at[y], y_dev(yq)).start()
                remote(t0s.at[yq], t0r.at[y], t0_send.at[yq], t0_recv.at[y], y_dev(yq)).start()

            return carry

        lax.fori_loop(0, ny, body, 0)

    for count in range(2, nz + 1, 2):
        pl.when(z // 2 == count // 2 - 1)(functools.partial(head0, count))
    o0r[y] = o0s[y]
    t0r[y] = t0s[y]

    def head1(zq, carry):
        unit(gz[zq, 0], gy, ny, lambda k: 0, ny, o1s.at[zq], t1s.at[zq])
        remote(o1s.at[zq], o1r.at[z], o1_send.at[zq], o1_recv.at[z], z_dev(zq)).start()
        remote(t1s.at[zq], t1r.at[z], t1_send.at[zq], t1_recv.at[z], z_dev(zq)).start()
        return carry

    lax.fori_loop(z + 1, nz, head1, 0)
    unit(gz[z, 0], gy, ny, lambda k: (y - k) * ROWS, 0, o1r.at[z], t1r.at[z])

    for d in range(1, ny):
        yy = (y + d) % ny
        remote(in_r.at[yy], in_r.at[yy], in_send.at[0], in_recv.at[yy], y_dev(yy)).wait_recv()
    rec = []
    for h in range(2):
        o = ol_scr[h] + dot_nt(qc_scr[h], in_r[:, h].reshape(DV, DV))
        rec.append(norm_rows(o, recg_ref[...]).astype(BF16))
    rec_rows = jnp.concatenate(rec, axis=1)

    def merge(o_ref, t_ref, k, carry):
        top, total, num = carry
        t_new = t_ref[k]
        now = jnp.maximum(top, t_new[0:1, :])
        old_w = jnp.exp(top - now)
        new_w = jnp.exp(t_new[0:1, :] - now)
        total = old_w * total + new_w * t_new[1:2, :]
        num = old_w * num + new_w * o_ref[k].astype(F32)
        return (now, total, num)

    start = (
        jnp.full((1, 2 * ROWS), NEG, F32), jnp.zeros((1, 2 * ROWS), F32), jnp.zeros((DV, 2 * ROWS), F32)
    )

    def finish(h, carry):
        top, total, num = carry
        att = num[:, :ROWS] / total[:, :ROWS] - lam_ref[h] * num[:, ROWS:] / total[:, ROWS:]
        att = att * lax.rsqrt(jnp.mean(att * att, axis=0, keepdims=True) + EPS)
        lws_ref[h:h + 1, :] = top[:, :ROWS] + jnp.log(total[:, :ROWS])
        return (att.T * attg_ref[...] * 0.8).astype(BF16)

    def merge0(k, carry):
        @pl.when(k != y)
        def _():
            remote(o0r.at[k], o0r.at[k], o0_send.at[0], o0_recv.at[k], y_dev(y)).wait_recv()
            remote(t0r.at[k], t0r.at[k], t0_send.at[0], t0_recv.at[k], y_dev(y)).wait_recv()

        return merge(o0r, t0r, k, carry)

    def merge1(k, carry):
        @pl.when(k != z)
        def _():
            remote(o1r.at[k], o1r.at[k], o1_send.at[0], o1_recv.at[k], z_dev(z)).wait_recv()
            remote(t1r.at[k], t1r.at[k], t1_send.at[0], t1_recv.at[k], z_dev(z)).wait_recv()

        return merge(o1r, t1r, k, carry)

    att0 = finish(0, lax.fori_loop(0, ny, merge0, start))
    att1 = finish(1, lax.fori_loop(0, z + 1, merge1, start))
    att_rows = jnp.concatenate([att0, att1], axis=1)

    for c in wo_copies:
        c.wait()
    width = wo.shape[2] // PARTS
    p_list = []
    for k in range(PARTS):
        cols = slice(k * width, (k + 1) * width)
        part = dot_nn(att_rows, wo[0, :, cols]) + dot_nn(rec_rows, wo[1, :, cols])
        pbuf[k] = part.astype(BF16)
        c = remote(pbuf.at[k], prx.at[k], p_send.at[k], p_recv.at[k], {"tp": t_other})
        c.start()
        p_list.append(c)
    for k in range(PARTS):
        p_list[k].wait_recv()
        out_ref[:, k * width:(k + 1) * width] = (pbuf[k].astype(F32) + prx[k].astype(F32)).astype(BF16)

    for c in a_list + r_list + g_list + p_list:
        c.wait_send()

    def sent0(k, carry):
        @pl.when(k != y)
        def _():
            remote(o0s.at[k], o0r.at[y], o0_send.at[k], o0_recv.at[y], y_dev(k)).wait_send()
            remote(t0s.at[k], t0r.at[y], t0_send.at[k], t0_recv.at[y], y_dev(k)).wait_send()

        return carry

    lax.fori_loop(0, ny, sent0, 0)

    def sent1(k, carry):
        remote(o1s.at[k], o1r.at[z], o1_send.at[k], o1_recv.at[z], z_dev(k)).wait_send()
        remote(t1s.at[k], t1r.at[z], t1_send.at[k], t1_recv.at[z], z_dev(k)).wait_send()
        return carry

    lax.fori_loop(z + 1, nz, sent1, 0)


def on_device(nz, ny, tokens, in_gain, wq, wk, wv, wrq, wrf, wri, lam, lb, scale, attg, recg, wa, wr):
    d = tokens.shape[1]
    out_cols = wa.shape[1]
    any_spec = pl.BlockSpec(memory_space=pl.ANY)
    vmem = pl.BlockSpec(memory_space=pltpu.VMEM)
    smem = pl.BlockSpec(memory_space=pltpu.SMEM)
    slice_rows = DV // ny
    st_rows = 2 * slice_rows + 16
    dma = pltpu.SemaphoreType.DMA
    scratch = [
        pltpu.VMEM((ROWS, d), BF16),
        pltpu.VMEM((6, d, DK), BF16),
        pltpu.VMEM((d, COLS), BF16),
        pltpu.VMEM((2, wa.shape[0], out_cols), BF16),
        pltpu.VMEM((FS, ROWS, d), BF16),
        pltpu.VMEM((FS, ROWS, COLS), BF16),
        pltpu.VMEM((3, ROWS, COLS), BF16),
        pltpu.VMEM((ny, 3, ROWS, DV), BF16),
        pltpu.VMEM((nz, 3, ROWS, DV), BF16),
        pltpu.VMEM((max(ny, nz), ROWS, 2 * ROWS), F32),
        pltpu.VMEM((8, 128), F32),
        pltpu.VMEM((ny, DV, 2 * ROWS), BF16),
        pltpu.VMEM((ny, DV, 2 * ROWS), BF16),
        pltpu.VMEM((ny, 8, 2 * ROWS), F32),
        pltpu.VMEM((ny, 8, 2 * ROWS), F32),
        pltpu.VMEM((nz, DV, 2 * ROWS), BF16),
        pltpu.VMEM((nz, DV, 2 * ROWS), BF16),
        pltpu.VMEM((nz, 8, 2 * ROWS), F32),
        pltpu.VMEM((nz, 8, 2 * ROWS), F32),
        pltpu.VMEM((ny, st_rows, DV), F32),
        pltpu.VMEM((ny, st_rows, DV), F32),
        pltpu.VMEM((st_rows, DV), F32),
        pltpu.VMEM((nz, st_rows, DV), F32),
        pltpu.VMEM((ny, 2, slice_rows, DV), BF16),
        pltpu.VMEM((ny, 2, slice_rows, DV), BF16),
        pltpu.VMEM((ny, st_rows, DV), F32),
        pltpu.VMEM((2, ROWS, DV), BF16),
        pltpu.VMEM((2, ROWS, DV), F32),
        pltpu.VMEM((PARTS, ROWS, out_cols // PARTS), BF16),
        pltpu.VMEM((PARTS, ROWS, out_cols // PARTS), BF16),
        dma((9,)), dma((12,)), dma((FS, 4)), dma((3,)), dma((FS,)),
        dma((ny,)), dma((ny,)), dma((nz,)), dma((nz,)),
        dma((ny,)), dma((ny,)), dma((ny,)), dma((ny,)),
        dma((nz,)), dma((nz,)), dma((nz,)), dma((nz,)),
        dma((ny,)), dma((ny,)), dma((nz,)), dma((nz,)), dma((ny,)), dma((ny,)),
        dma((PARTS,)), dma((PARTS,)),
    ]
    return pl.pallas_call(
        functools.partial(kernel_body, nz, ny),
        out_shape=(
            jax.ShapeDtypeStruct((ROWS, out_cols), BF16),
            jax.ShapeDtypeStruct((2, ROWS), F32),
        ),
        in_specs=[any_spec, vmem] + [any_spec] * 6 + [smem, vmem, vmem, vmem, vmem, any_spec, any_spec],
        out_specs=(vmem, vmem),
        scratch_shapes=scratch,
        compiler_params=pltpu.CompilerParams(
            collective_id=0, has_side_effects=True, vmem_limit_bytes=56 * 1024 * 1024
        ),
    )(
        tokens, in_gain.reshape(1, d), wq, wk, wv, wrq, wrf, wri, lam, lb,
        scale.reshape(1, ROWS), attg.reshape(1, DV), recg.reshape(1, DV), wa, wr,
    )


def solution(mesh):
    sp = mesh.shape["sp"]
    nz = 1
    while nz * nz < sp:
        nz *= 2
    ny = sp // nz
    col_split = P(None, ("tp", "fs"))
    placed = (
        P(("fs", "sp"), None), P(),
        col_split, col_split, col_split, col_split, col_split, col_split,
        P("tp"), P("tp", None), P(("fs", "sp")), P(), P(),
        P("tp", None), P("tp", None),
    )
    return jax.shard_map(
        functools.partial(on_device, nz, ny),
        mesh=mesh,
        in_specs=placed,
        out_specs=(P(("fs", "sp"), None), P("tp", ("fs", "sp"))),
        check_vma=False,
    )
```

time: 368 us -> 94.1 us (0.26)
  waiting for transfers between devices: 228 us -> 0 us
  Pallas kernels: 0 us -> 83.7 us
  matrix products: 44.4 us -> 0 us
  blocking collectives: 31 us -> 0 us
  local copies, waits for them, and re-layouts: 33.7 us -> 9.51 us
  other arithmetic: 14.5 us -> 0 us
  between operations: 14.8 us -> 0.66 us
    all_gather x4 -> x0, waiting for transfers between devices: 228 us -> none  [the longest x1 102 us: in_one_piece(): filled = lax.all_gather(both, axis, axis=dim, tiled=True)]
    pallas_call x0 -> x1, Pallas kernels: none -> 83.7 us  [on_device(): pl.pallas_call(functools.partial(kernel_body, nz, ny), out_shape=(jax.Sha...]
    dot_general x14 -> x0, matrix products: 44.4 us -> none  [the longest x2 13.9 us: advance(): jnp.einsum('htk,htsk,hsk->hts', query_block, decay, key_block, precision=...]
    all_gather x2 -> x0, blocking collectives: 25.9 us -> none  [entering(): pieces = jax.tree.map(lambda part: lax.all_gather(part, axis), running)]
    another operation x2 -> x0, local copies, waits for them, and re-layouts: 12.9 us -> none
    reduce_sum x4 -> x0, other arithmetic: 9.47 us -> none  [the longest x1 8.07 us: attend(): weight_sum = jnp.sum(weights, axis=-1)]
    reshape x3 -> x0, local copies, waits for them, and re-layouts: 6.43 us -> none  [the longest x1 6.32 us: attend(): pair_values.reshape(key_rows, local_heads, DV).transpose(1, 0, 2)]
    split x1 -> x0, local copies, waits for them, and re-layouts: 5.94 us -> none  [in_one_piece(): jnp.split(filled, [sum(widths[:k]) for k in range(1, len(widths))], axis=...]
  transfers between devices with their start and end apart: 4 -> 0, of which waited for: 4 -> 0; matrix products, arithmetic and copies ran while one was open for 1% -> 0% of each run, Pallas kernels for 0% -> 0%
where the time goes in v1:
time: 94.1 us; the launch traced here: 93.9 us
  Pallas kernels  83.7 us (89%)
  local copies, waits for them, and re-layouts  9.51 us (10%)
    pallas_call x1, Pallas kernels, on_device(): pl.pallas_call(functools.partial(kernel_body, nz, ny), out_shape=(jax.Sha...  83.7 us
    unnamed x20, local copies, waits for them, and re-layouts  9.51 us

profile of v1, /device:TPU:1, one launch (start us, length us, event | category | flops | bytes accessed | tf_op | source)
XLA Modules:
  0.0 93.9 jit_solution(1026620368803331583)
XLA Ops:
  0.6 0.0 copy-start
  0.6 2.0 %copy.17.wq = bf16[2048,64]{1,0:T(8,128)(2,1)} copy(bf16[2048,64]{0,1:T(8,128)(2,1)} %param.17) | data formatting | bytes 524288 | tf_op args[2]
  2.6 0.0 copy-done
  2.6 0.0 copy-start.1
  2.6 1.0 %copy.18.wk = bf16[2048,64]{1,0:T(8,128)(2,1)} copy(bf16[2048,64]{0,1:T(8,128)(2,1)S(1)} %copy-done) | data formatting | bytes 524288 | tf_op args[3]
  3.6 0.0 copy-done.1
  3.6 0.0 copy-start.2
  3.6 1.0 %copy.19.wv = bf16[2048,64]{1,0:T(8,128)(2,1)} copy(bf16[2048,64]{0,1:T(8,128)(2,1)S(1)} %copy-done.1) | data formatting | bytes 524288 | tf_op args[4]
  4.7 0.0 copy-done.2
  4.7 0.0 copy-start.3
  4.7 1.0 %copy.20.wrq = bf16[2048,64]{1,0:T(8,128)(2,1)} copy(bf16[2048,64]{0,1:T(8,128)(2,1)S(1)} %copy-done.2) | data formatting | bytes 524288 | tf_op args[5]
  5.7 0.0 copy-done.3
  5.7 0.0 copy-start.4
  5.7 1.0 %copy.21.wrf = bf16[2048,64]{1,0:T(8,128)(2,1)} copy(bf16[2048,64]{0,1:T(8,128)(2,1)S(1)} %copy-done.3) | data formatting | bytes 524288 | tf_op args[6]
  6.7 0.0 copy-done.4
  6.7 1.0 %copy.22.wri = bf16[2048,64]{1,0:T(8,128)(2,1)} copy(bf16[2048,64]{0,1:T(8,128)(2,1)S(1)} %copy-done.4) | data formatting | bytes 524288 | tf_op args[7]
  7.7 83.7 %shard_map.158 = (bf16[128,2048]{1,0:T(8,128)(2,1)}, f32[2,128]{1,0:T(2,128)}) custom-call(bf16[128,2048]{1,0:T(8,128)(2,1)} %tok_hbm.1, f32[1,2048]{1,0:T(1,128)} %bitcast.4, bf16[2048,64]{1,0:T(8,128)(2,1)} %copy.17.wq, bf16[2048,64]{1,0:T(8,128)(2,1)} %copy.18.wk, bf16[2048,64]{1,0:T(8,128)(2,1)} %copy.19.wv, bf16[2048,64]{1,0:T(8,128)(2,1)} %copy.20.wrq, ...), custom_call_target="tpu_custom_call" | custom-call | tf_op jit(solution)/shard_map/pallas_call | solution.py:487
  91.4 0.0 copy-start.5
  91.4 1.9 %copy.25 = bf16[128,2048]{1,0:T(8,128)(2,1)} copy(bf16[128,2048]{1,0:T(8,128)(2,1)} %get-tuple-element.4) | data formatting | bytes 1048576
  93.3 0.0 copy-done.5
  93.3 0.6 copy.26
Async XLA Ops:
  0.6 2.0 %copy-start = (bf16[2048,64]{0,1:T(8,128)(2,1)S(1)}, bf16[2048,64]{0,1:T(8,128)(2,1)}, u32[]{:S(2)}) copy-start(bf16[2048,64]{0,1:T(8,128)(2,1)} %param.18) | copy-start | bytes 786436
  2.6 1.0 %copy-start.1 = (bf16[2048,64]{0,1:T(8,128)(2,1)S(1)}, bf16[2048,64]{0,1:T(8,128)(2,1)}, u32[]{:S(2)}) copy-start(bf16[2048,64]{0,1:T(8,128)(2,1)} %param.19) | copy-start | bytes 786436
  3.6 1.0 %copy-start.2 = (bf16[2048,64]{0,1:T(8,128)(2,1)S(1)}, bf16[2048,64]{0,1:T(8,128)(2,1)}, u32[]{:S(2)}) copy-start(bf16[2048,64]{0,1:T(8,128)(2,1)} %param.20) | copy-start | bytes 786436
  4.7 1.0 %copy-start.3 = (bf16[2048,64]{0,1:T(8,128)(2,1)S(1)}, bf16[2048,64]{0,1:T(8,128)(2,1)}, u32[]{:S(2)}) copy-start(bf16[2048,64]{0,1:T(8,128)(2,1)} %param.21) | copy-start | bytes 786436
  5.7 1.0 %copy-start.4 = (bf16[2048,64]{0,1:T(8,128)(2,1)S(1)}, bf16[2048,64]{0,1:T(8,128)(2,1)}, u32[]{:S(2)}) copy-start(bf16[2048,64]{0,1:T(8,128)(2,1)} %param.22) | copy-start | bytes 786436
  91.4 1.9 %copy-start.5 = (f32[2,128]{1,0:T(2,128)S(1)}, f32[2,128]{1,0:T(2,128)}, u32[]{:S(2)}) copy-start(f32[2,128]{1,0:T(2,128)} %get-tuple-element.5) | copy-start | bytes 3076

commit v2 on v1

--- a/solution.py
+++ b/solution.py
@@ -28,6 +28,19 @@
     return lax.dot_general(a, b, (((1,), (1,)), ((), ())), preferred_element_type=F32)
 
 
+def pack_rates(first, second):
+    parts = []
+    for rate in (first, second):
+        high = rate.astype(BF16).astype(F32)
+        parts += [jnp.broadcast_to(v, (4, DV)) for v in (high, rate - high)]
+    return jnp.concatenate(parts, axis=0).astype(BF16)
+
+
+def unpack_rates(packed):
+    wide = packed.astype(F32)
+    return wide[0:1] + wide[4:5], wide[8:9] + wide[12:13]
+
+
 def norm_rows(values, gain):
     mean = jnp.mean(values * values, axis=-1, keepdims=True)
     return values * lax.rsqrt(mean + EPS) * gain
@@ -38,8 +51,8 @@
     tok_hbm, gain_ref, wq, wk, wv, wrq, wrf, wri, lam_ref, lb_ref, scale_ref, attg_ref, recg_ref,
     wa_hbm, wr_hbm,
     out_ref, lws_ref,
-    tok, wraw, wcat, wo, nrm, res, rsend,
-    gy, gz, s_scr, e_scr,
+    tok, wcat, wo, nrm, res, rsend,
+    gy, gz, s_scr, e_scr, vt,
     o0s, o0r, t0s, t0r, o1s, o1r, t1s, t1r,
     st_s, st_r, tot_s, tot_r, in_s, in_r, pref, qc_scr, ol_scr,
     pbuf, prx,
@@ -60,10 +73,23 @@
     xo = (x + 2) % 4
     slice_rows = DV // ny
 
+    open_scope = []
+
+    def phase(name):
+        if open_scope:
+            open_scope.pop().__exit__(None, None, None)
+        if name:
+            scope = jax.named_scope(name)
+            scope.__enter__()
+            open_scope.append(scope)
+
+    phase("start")
     weights = (wq, wk, wv, wrq, wrf, wri)
     tok_copy = pltpu.make_async_copy(tok_hbm, tok, lsem.at[0])
     tok_copy.start()
-    w_copies = [pltpu.make_async_copy(w, wraw.at[i], lsem.at[1 + i]) for i, w in enumerate(weights)]
+    w_copies = [
+        pltpu.make_async_copy(w, wcat.at[pl.ds(i * DK, DK)], lsem.at[1 + i]) for i, w in enumerate(weights)
+    ]
     for c in w_copies:
         c.start()
     wo_copies = [
@@ -104,6 +130,7 @@
     tok_copy.wait()
     normalise(t, 0)
     normalise(t, 1)
+    phase("entry_barrier")
     pl.semaphore_wait(barrier, 1 + 3 + (ny - 1) + (nz - 1))
 
     a_list = []
@@ -116,6 +143,7 @@
     def a_wait(f, tt, pc):
         remote(piece(f, tt, pc), piece(f, tt, pc), a_send.at[0], a_sem(f, tt, pc), {"fs": xr}).wait_recv()
 
+    phase("x_own")
     a_start(0, x, 0, {"fs": xr})
     a_start(1, x, 1, {"fs": xl})
     a_start(2, x, 1, {"fs": xr})
@@ -124,12 +152,12 @@
     normalise(t_other, 1)
     for i in range(6):
         w_copies[i].wait()
-        wcat[:, i * 64:(i + 1) * 64] = wraw[i]
 
     def project(f):
-        return dot_nn(nrm[f], wcat[...]).astype(BF16)
+        return dot_nt(nrm[f], wcat[...]).astype(BF16)
 
     res[x] = project(x)
+    phase("x_forward")
     a_wait(xl, t, 0)
     a_start(4, xl, 0, {"fs": xr})
     a_start(5, xl, 0, {"tp": t_other})
@@ -151,16 +179,20 @@
         c.start()
         r_list.append(c)
 
+    phase("x_near")
     answer(0, xl)
     answer(1, xr)
+    phase("x_far")
     a_wait(xo, t, 0)
     a_start(10, xo, 0, {"tp": t_other})
     a_wait(xo, t, 1)
     a_start(11, xo, 1, {"tp": t_other})
     answer(2, xo)
+    phase("x_answers")
     for f in (xl, xr, xo):
         remote(res.at[f], res.at[f], r_send.at[0], r_recv.at[f], {"fs": xr}).wait_recv()
 
+    phase("tiles")
     def tile(kind, h):
         lo = kind * 64
         return jnp.concatenate([res[2 * h, :, lo:lo + 64], res[2 * h + 1, :, lo:lo + 64]], axis=1)
@@ -183,19 +215,36 @@
         return {"sp": zz * ny + y}
 
     g_list = []
-    for d in range(1, max(ny, nz)):
-        if d < ny:
-            c = remote(gy.at[y], gy.at[y], gy_send.at[d], gy_recv.at[y], y_dev((y + d) % ny))
-            c.start()
-            g_list.append(c)
-        if d < nz:
-            c = remote(gz.at[z], gz.at[z], gz_send.at[d], gz_recv.at[z], z_dev((z + d) % nz))
-            c.start()
-            g_list.append(c)
-
+
+    def tile_copy(buf, sent, got, slot, k, dev, way, hop):
+        return remote(buf.at[slot, k], buf.at[slot, k], sent.at[way, hop, k], got.at[slot, k], dev)
+
+    def pass_on(hop):
+        for k in range(3):
+            for buf, sent, got, me, size, dev in (
+                (gy, gy_send, gy_recv, y, ny, y_dev), (gz, gz_send, gz_recv, z, nz, z_dev)
+            ):
+                for side, way in enumerate((1, -1)):
+                    def carried(h):
+                        return 2 * h < size or (2 * h == size and (k % 2 == 0) == (way == 1))
+
+                    if not (hop > 0 and carried(hop)) and not carried(hop + 1):
+                        continue
+                    slot = (me + size - way * hop) % size
+                    c = tile_copy(buf, sent, got, slot, k, dev((me + size + way) % size), side, hop)
+                    if hop > 0 and carried(hop):
+                        c.wait_recv()
+                    if carried(hop + 1):
+                        c.start()
+                        g_list.append(c)
+
+    pass_on(0)
+
+    phase("rec_local")
     row = lax.broadcasted_iota(jnp.int32, (ROWS, ROWS), 0)
     col = lax.broadcasted_iota(jnp.int32, (ROWS, ROWS), 1)
     tril = jnp.where(row >= col, 1.0, 0.0).astype(F32)
+    rates = []
     scale_col = jnp.broadcast_to(scale_ref[...], (ROWS, ROWS)).T
     for h in range(2):
         rq = tile(3, h).astype(F32)
@@ -231,10 +280,11 @@
         key_end = (kk * jnp.exp(last - cum)).astype(BF16)
         state_t = dot_nn(ri.astype(F32).T.astype(BF16), key_end)
         qc_scr[h] = (rq * jnp.exp(cum)).astype(BF16)
-        st_s[:, h * slice_rows:(h + 1) * slice_rows, :] = state_t.reshape(ny, slice_rows, DV)
-        st_s[:, 2 * slice_rows + 8 * h:2 * slice_rows + 8 * h + 8, :] = jnp.broadcast_to(
-            jnp.exp(last).reshape(1, 1, DV), (ny, 8, DV)
-        )
+        st_s[:, h * slice_rows:(h + 1) * slice_rows, :] = state_t.reshape(ny, slice_rows, DV).astype(BF16)
+        rates.append(jnp.exp(last))
+    packed = pack_rates(*rates)
+    for k in range(ny):
+        st_s[k, 2 * slice_rows:, :] = packed
     st_r[y] = st_s[y]
     for d in range(1, ny):
         yy = (y + d) % ny
@@ -242,36 +292,46 @@
         c.start()
         g_list.append(c)
 
+    phase("gather_near")
+    far_hop = min(3, max(ny, nz) // 2)
+    for hop in range(1, far_hop):
+        pass_on(hop)
+    phase("rec_prefix")
     for d in range(1, ny):
         yy = (y + d) % ny
         remote(st_r.at[yy], st_r.at[yy], st_send.at[0], st_recv.at[yy], y_dev(yy)).wait_recv()
     half = slice_rows
-    for h in range(2):
-        state = jnp.zeros((half, DV), F32)
-        rate = jnp.ones((8, DV), F32)
-        for k in range(ny):
-            pref[k, h * half:(h + 1) * half, :] = state
-            pref[k, 2 * half + 8 * h:2 * half + 8 * h + 8, :] = rate
-            step = st_r[k, 2 * half + 8 * h:2 * half + 8 * h + 8, :]
-            state = step[0:1, :] * state + st_r[k, h * half:(h + 1) * half, :]
-            rate = rate * step
-        tot_s[h * half:(h + 1) * half, :] = state
-        tot_s[2 * half + 8 * h:2 * half + 8 * h + 8, :] = rate
+
+    def step_of(ref):
+        d0, d1 = unpack_rates(ref[2 * half:, :])
+        return d0, ref[0:half, :].astype(F32), d1, ref[half:2 * half, :].astype(F32)
+
+    s0 = s1 = jnp.zeros((half, DV), F32)
+    c0 = c1 = jnp.ones((1, DV), F32)
+    for k in range(ny):
+        pref[k, 0:half, :] = s0
+        pref[k, half:2 * half, :] = s1
+        pref[k, 2 * half:2 * half + 8, :] = jnp.broadcast_to(c0, (8, DV))
+        pref[k, 2 * half + 8:2 * half + 16, :] = jnp.broadcast_to(c1, (8, DV))
+        d0, a0, d1, a1 = step_of(st_r.at[k])
+        s0, s1, c0, c1 = d0 * s0 + a0, d1 * s1 + a1, c0 * d0, c1 * d1
+    tot_s[0:half, :] = s0.astype(BF16)
+    tot_s[half:2 * half, :] = s1.astype(BF16)
+    tot_s[2 * half:, :] = pack_rates(c0, c1)
     for d in range(1, nz):
         zz = (z + d) % nz
         c = remote(tot_s, tot_r.at[z], tot_send.at[d], tot_recv.at[z], z_dev(zz))
         c.start()
         g_list.append(c)
 
+    phase("rec_totals")
     for d in range(1, nz):
         zz = (z + d) % nz
         remote(tot_r.at[zz], tot_r.at[zz], tot_send.at[0], tot_recv.at[zz], z_dev(zz)).wait_recv()
 
     def fold(k, carry):
-        s0, s1 = carry
-        d0 = tot_r[k, 2 * half:2 * half + 1, :]
-        d1 = tot_r[k, 2 * half + 8:2 * half + 9, :]
-        return (d0 * s0 + tot_r[k, 0:half, :], d1 * s1 + tot_r[k, half:2 * half, :])
+        d0, a0, d1, a1 = step_of(tot_r.at[k])
+        return (d0 * carry[0] + a0, d1 * carry[1] + a1)
 
     entry = lax.fori_loop(0, z, fold, (jnp.zeros((half, DV), F32), jnp.zeros((half, DV), F32)))
     for k in range(ny):
@@ -285,72 +345,84 @@
         c.start()
         g_list.append(c)
 
-    for d in range(1, ny):
-        yy = (y + d) % ny
-        remote(gy.at[yy], gy.at[yy], gy_send.at[0], gy_recv.at[yy], y_dev(yy)).wait_recv()
-    for d in range(1, nz):
-        zz = (z + d) % nz
-        remote(gz.at[zz], gz.at[zz], gz_send.at[0], gz_recv.at[zz], z_dev(zz)).wait_recv()
-
+    phase("gather_wait")
+    for hop in range(far_hop, max(ny, nz) // 2 + 1):
+        pass_on(hop)
+
+    phase("att_head0")
     lane = lax.broadcasted_iota(jnp.int32, (ROWS, DV), 1)
 
-    def unit(queries, tiles, count, limits, masked_from, o_out, t_out):
+    def unit(queries, tiles, count, limits, masked_from, o_out, t_out, lane_slot):
         zero = jnp.zeros_like(queries)
         both = jnp.concatenate(
             [jnp.where(lane < DK, queries, zero), jnp.where(lane < DK, zero, queries)], axis=0
         )
+        keys = count * ROWS
+        s_scr[lane_slot, :keys, :] = dot_nt(tiles[:count, 1].reshape(keys, DV), both)
         top = jnp.full((8, 2 * ROWS), NEG, F32)
         for k in range(count):
-            s = dot_nt(tiles[k, 1], both)
+            rows = slice(k * ROWS, (k + 1) * ROWS)
+            s = s_scr[lane_slot, rows, :]
             if k >= masked_from:
                 ri_ = lax.broadcasted_iota(jnp.int32, (ROWS, 2 * ROWS), 0)
                 ci_ = lax.broadcasted_iota(jnp.int32, (ROWS, 2 * ROWS), 1) & (ROWS - 1)
                 s = jnp.where(ri_ - ci_ <= limits(k), s, NEG)
-            s_scr[k] = s
+                s_scr[lane_slot, rows, :] = s
             top = jnp.maximum(top, jnp.max(s.reshape(ROWS // 8, 8, 2 * ROWS), axis=0))
         top = jnp.max(top, axis=0, keepdims=True)
         total = jnp.zeros((8, 2 * ROWS), F32)
-        num = jnp.zeros((DV, 2 * ROWS), F32)
         for k in range(count):
-            e = jnp.exp(s_scr[k] - top)
+            rows = slice(k * ROWS, (k + 1) * ROWS)
+            e = jnp.exp(s_scr[lane_slot, rows, :] - top)
             total = total + jnp.sum(e.reshape(ROWS // 8, 8, 2 * ROWS), axis=0)
-            num = num + dot_nn(tiles[k, 2], e.astype(BF16))
-        total = jnp.sum(total, axis=0, keepdims=True)
+            e_scr[lane_slot, rows, :] = e.astype(BF16)
+        num = dot_nn(vt[:, :keys], e_scr[lane_slot, :keys, :])
         o_out[...] = num.astype(BF16)
         t_out[0:1, :] = top
-        t_out[1:2, :] = total
+        t_out[1:2, :] = jnp.sum(total, axis=0, keepdims=True)
 
     def head0(count):
-        def body(yq, carry):
-            unit(
-                gy[yq, 0], gz, count,
-                lambda k: ((z - k) * ny + (yq - y)) * ROWS,
-                count - 2, o0s.at[yq], t0s.at[yq],
-            )
-
-            @pl.when(yq != y)
-            def _():
-                remote(o0s.at[yq], o0r.at[y], o0_send.at[yq], o0_recv.at[y], y_dev(yq)).start()
-                remote(t0s.at[yq], t0r.at[y], t0_send.at[yq], t0_recv.at[y], y_dev(yq)).start()
+        for k in range(count):
+            vt[:, k * ROWS:(k + 1) * ROWS] = gz[k, 2]
+
+        def body(i, carry):
+            blocks = [(y + ny // 2 + i) % ny, (y + 2 * ny - 1 - i - ny // 2) % ny]
+            for j, yq in enumerate(blocks):
+                unit(
+                    gy[yq, 0], gz, count,
+                    lambda k, yq=yq: ((z - k) * ny + (yq - y)) * ROWS,
+                    count - 2, o0s.at[yq], t0s.at[yq], j,
+                )
+            for yq in blocks:
+                @pl.when(yq != y)
+                def _():
+                    remote(o0s.at[yq], o0r.at[y], o0_send.at[yq], o0_recv.at[y], y_dev(yq)).start()
+                    remote(t0s.at[yq], t0r.at[y], t0_send.at[yq], t0_recv.at[y], y_dev(yq)).start()
 
             return carry
 
-        lax.fori_loop(0, ny, body, 0)
+        lax.fori_loop(0, ny // 2, body, 0)
 
     for count in range(2, nz + 1, 2):
         pl.when(z // 2 == count // 2 - 1)(functools.partial(head0, count))
     o0r[y] = o0s[y]
     t0r[y] = t0s[y]
 
-    def head1(zq, carry):
-        unit(gz[zq, 0], gy, ny, lambda k: 0, ny, o1s.at[zq], t1s.at[zq])
+    phase("att_head1")
+    for k in range(ny):
+        vt[:, k * ROWS:(k + 1) * ROWS] = gy[k, 2]
+
+    def head1(i, carry):
+        zq = nz - 1 - i
+        unit(gz[zq, 0], gy, ny, lambda k: 0, ny, o1s.at[zq], t1s.at[zq], 0)
         remote(o1s.at[zq], o1r.at[z], o1_send.at[zq], o1_recv.at[z], z_dev(zq)).start()
         remote(t1s.at[zq], t1r.at[z], t1_send.at[zq], t1_recv.at[z], z_dev(zq)).start()
         return carry
 
-    lax.fori_loop(z + 1, nz, head1, 0)
-    unit(gz[z, 0], gy, ny, lambda k: (y - k) * ROWS, 0, o1r.at[z], t1r.at[z])
-
+    lax.fori_loop(0, nz - 1 - z, head1, 0)
+    unit(gz[z, 0], gy, ny, lambda k: (y - k) * ROWS, 0, o1r.at[z], t1r.at[z], 0)
+
+    phase("rec_result")
     for d in range(1, ny):
         yy = (y + d) % ny
         remote(in_r.at[yy], in_r.at[yy], in_send.at[0], in_recv.at[yy], y_dev(yy)).wait_recv()
@@ -360,6 +432,7 @@
         rec.append(norm_rows(o, recg_ref[...]).astype(BF16))
     rec_rows = jnp.concatenate(rec, axis=1)
 
+    phase("merge_start")
     def merge(o_ref, t_ref, k, carry):
         top, total, num = carry
         t_new = t_ref[k]
@@ -397,10 +470,13 @@
 
         return merge(o1r, t1r, k, carry)
 
+    phase("merge_zero")
     att0 = finish(0, lax.fori_loop(0, ny, merge0, start))
+    phase("merge_one")
     att1 = finish(1, lax.fori_loop(0, z + 1, merge1, start))
     att_rows = jnp.concatenate([att0, att1], axis=1)
 
+    phase("project_out")
     for c in wo_copies:
         c.wait()
     width = wo.shape[2] // PARTS
@@ -416,6 +492,7 @@
         p_list[k].wait_recv()
         out_ref[:, k * width:(k + 1) * width] = (pbuf[k].astype(F32) + prx[k].astype(F32)).astype(BF16)
 
+    phase("drain")
     for c in a_list + r_list + g_list + p_list:
         c.wait_send()
 
@@ -435,6 +512,12 @@
         return carry
 
     lax.fori_loop(z + 1, nz, sent1, 0)
+    phase(None)
+
+
+def hand_over(mixed_ref, log_ref, mixed_out, log_out):
+    mixed_out[...] = mixed_ref[...]
+    log_out[...] = log_ref[...]
 
 
 def on_device(nz, ny, tokens, in_gain, wq, wk, wv, wrq, wrf, wri, lam, lb, scale, attg, recg, wa, wr):
@@ -448,16 +531,16 @@
     dma = pltpu.SemaphoreType.DMA
     scratch = [
         pltpu.VMEM((ROWS, d), BF16),
-        pltpu.VMEM((6, d, DK), BF16),
-        pltpu.VMEM((d, COLS), BF16),
+        pltpu.VMEM((COLS, d), BF16),
         pltpu.VMEM((2, wa.shape[0], out_cols), BF16),
         pltpu.VMEM((FS, ROWS, d), BF16),
         pltpu.VMEM((FS, ROWS, COLS), BF16),
         pltpu.VMEM((3, ROWS, COLS), BF16),
         pltpu.VMEM((ny, 3, ROWS, DV), BF16),
         pltpu.VMEM((nz, 3, ROWS, DV), BF16),
-        pltpu.VMEM((max(ny, nz), ROWS, 2 * ROWS), F32),
-        pltpu.VMEM((8, 128), F32),
+        pltpu.VMEM((2, max(ny, nz) * ROWS, 2 * ROWS), F32),
+        pltpu.VMEM((2, max(ny, nz) * ROWS, 2 * ROWS), BF16),
+        pltpu.VMEM((DV, max(ny, nz) * ROWS), BF16),
         pltpu.VMEM((ny, DV, 2 * ROWS), BF16),
         pltpu.VMEM((ny, DV, 2 * ROWS), BF16),
         pltpu.VMEM((ny, 8, 2 * ROWS), F32),
@@ -466,10 +549,10 @@
         pltpu.VMEM((nz, DV, 2 * ROWS), BF16),
         pltpu.VMEM((nz, 8, 2 * ROWS), F32),
         pltpu.VMEM((nz, 8, 2 * ROWS), F32),
-        pltpu.VMEM((ny, st_rows, DV), F32),
-        pltpu.VMEM((ny, st_rows, DV), F32),
-        pltpu.VMEM((st_rows, DV), F32),
-        pltpu.VMEM((nz, st_rows, DV), F32),
+        pltpu.VMEM((ny, st_rows, DV), BF16),
+        pltpu.VMEM((ny, st_rows, DV), BF16),
+        pltpu.VMEM((st_rows, DV), BF16),
+        pltpu.VMEM((nz, st_rows, DV), BF16),
         pltpu.VMEM((ny, 2, slice_rows, DV), BF16),
         pltpu.VMEM((ny, 2, slice_rows, DV), BF16),
         pltpu.VMEM((ny, st_rows, DV), F32),
@@ -478,13 +561,13 @@
         pltpu.VMEM((PARTS, ROWS, out_cols // PARTS), BF16),
         pltpu.VMEM((PARTS, ROWS, out_cols // PARTS), BF16),
         dma((9,)), dma((12,)), dma((FS, 4)), dma((3,)), dma((FS,)),
-        dma((ny,)), dma((ny,)), dma((nz,)), dma((nz,)),
+        dma((2, ny // 2 + 1, 3)), dma((ny, 3)), dma((2, nz // 2 + 1, 3)), dma((nz, 3)),
         dma((ny,)), dma((ny,)), dma((ny,)), dma((ny,)),
         dma((nz,)), dma((nz,)), dma((nz,)), dma((nz,)),
         dma((ny,)), dma((ny,)), dma((nz,)), dma((nz,)), dma((ny,)), dma((ny,)),
         dma((PARTS,)), dma((PARTS,)),
     ]
-    return pl.pallas_call(
+    mixed, log_sum = pl.pallas_call(
         functools.partial(kernel_body, nz, ny),
         out_shape=(
             jax.ShapeDtypeStruct((ROWS, out_cols), BF16),
@@ -497,9 +580,18 @@
             collective_id=0, has_side_effects=True, vmem_limit_bytes=56 * 1024 * 1024
         ),
     )(
-        tokens, in_gain.reshape(1, d), wq, wk, wv, wrq, wrf, wri, lam, lb,
+        tokens, in_gain.reshape(1, d), wq.T, wk.T, wv.T, wrq.T, wrf.T, wri.T, lam, lb,
         scale.reshape(1, ROWS), attg.reshape(1, DV), recg.reshape(1, DV), wa, wr,
     )
+    return pl.pallas_call(
+        hand_over,
+        out_shape=(
+            jax.ShapeDtypeStruct((ROWS, out_cols), BF16),
+            jax.ShapeDtypeStruct((2, ROWS), F32),
+        ),
+        in_specs=[vmem, vmem],
+        out_specs=(vmem, vmem),
+    )(mixed, log_sum)
 
 
 def solution(mesh):

time: 94.1 us -> 75.9 us (0.81)
  local copies, waits for them, and re-layouts: 9.51 us -> 0 us
  Pallas kernels: 83.7 us -> 75.1 us
    pallas_call x1, Pallas kernels: 83.7 us -> 73.2 us  [on_device(): pl.pallas_call(functools.partial(kernel_body, nz, ny), out_shape=(jax.Sha...]
    unnamed x20 -> x0, local copies, waits for them, and re-layouts: 9.51 us -> none
    pallas_call x0 -> x1, Pallas kernels: none -> 1.87 us  [on_device(): pl.pallas_call(hand_over, out_shape=(jax.ShapeDtypeStruct((ROWS, out_cols...]
where the time goes in v2:
time: 75.9 us; the launch traced here: 75.7 us
  Pallas kernels  75.1 us (99%)
    pallas_call x1, Pallas kernels, on_device(): pl.pallas_call(functools.partial(kernel_body, nz, ny), out_shape=(jax.Sha...  73.2 us
    pallas_call x1, Pallas kernels, on_device(): pl.pallas_call(hand_over, out_shape=(jax.ShapeDtypeStruct((ROWS, out_cols...  1.87 us

profile of v2, /device:TPU:1, one launch (start us, length us, event | category | flops | bytes accessed | tf_op | source)
XLA Modules:
  0.0 75.7 jit_solution(1152035066561045737)
XLA Ops:
  0.6 73.2 %shard_map.158 = (bf16[128,2048]{1,0:T(8,128)(2,1)}, f32[2,128]{1,0:T(2,128)}) custom-call(bf16[128,2048]{1,0:T(8,128)(2,1)} %tok_hbm.1, f32[1,2048]{1,0:T(1,128)} %bitcast.16, bf16[64,2048]{1,0:T(8,128)(2,1)} %bitcast.10, bf16[64,2048]{1,0:T(8,128)(2,1)} %bitcast.11, bf16[64,2048]{1,0:T(8,128)(2,1)} %bitcast.12, bf16[64,2048]{1,0:T(8,128)(2,1)} %bitcast.13, ...), custom_call_target="tpu_custom_call" | custom-call | tf_op jit(solution)/shard_map/pallas_call | solution.py:570
  73.9 1.9 %shard_map.159 = (bf16[128,2048]{1,0:T(8,128)(2,1)}, f32[2,128]{1,0:T(2,128)}) custom-call(bf16[128,2048]{1,0:T(8,128)(2,1)} %get-tuple-element.4.mixed_ref, f32[2,128]{1,0:T(2,128)} %get-tuple-element.5.log_ref), custom_call_target="tpu_custom_call" | custom-call | tf_op jit(solution)/shard_map/pallas_call | solution.py:586

commit v3 on v2

v3 whole, which is shorter than its diff:
```python
import functools

import jax
import jax.numpy as jnp
from jax import lax
from jax.experimental import pallas as pl
from jax.experimental.pallas import tpu as pltpu
from jax.sharding import PartitionSpec as P

DK = 64
DV = 128
ROWS = 128
COLS = 384
FIRST = 256
EPS = 1e-06
NEG = -1e30
FS = 4
PARTS = 4
MESH = pl.DeviceIdType.MESH
F32 = jnp.float32
BF16 = jnp.bfloat16


def dot_nn(a, b):
    return lax.dot_general(a, b, (((1,), (0,)), ((), ())), preferred_element_type=F32)


def dot_nt(a, b):
    return lax.dot_general(a, b, (((1,), (1,)), ((), ())), preferred_element_type=F32)


def pack_rates(first, second):
    parts = []
    for rate in (first, second):
        high = rate.astype(BF16).astype(F32)
        parts += [jnp.broadcast_to(v, (4, DV)) for v in (high, rate - high)]
    return jnp.concatenate(parts, axis=0).astype(BF16)


def unpack_rates(packed):
    wide = packed.astype(F32)
    return wide[0:1] + wide[4:5], wide[8:9] + wide[12:13]


def pack_stats(rows):
    tile = jnp.zeros((16, DV), F32)
    where = lax.broadcasted_iota(jnp.int32, (16, DV), 0)
    for i, value in enumerate(rows):
        high = value.astype(BF16).astype(F32)
        middle = (value - high).astype(BF16).astype(F32)
        for j, part in enumerate((high, middle, value - high - middle)):
            tile = jnp.where(where == 3 * i + j, part, tile)
    return tile.astype(BF16)


def unpack_stats(packed):
    wide = packed.astype(F32)
    return [wide[3 * i:3 * i + 1] + wide[3 * i + 1:3 * i + 2] + wide[3 * i + 2:3 * i + 3] for i in range(4)]


def norm_rows(values, gain):
    mean = jnp.mean(values * values, axis=-1, keepdims=True)
    return values * lax.rsqrt(mean + EPS) * gain


def kernel_body(
    nz, ny,
    tok_hbm, gain_ref, wq, wk, wv, wrq, wrf, wri, lam_ref, lb_ref, scale_ref, attg_ref, recg_ref,
    wa_hbm, wr_hbm,
    out_ref, lws_ref,
    tok, wcat, wo, nrm, res, res2, rsend, rsend2,
    gy, gz, acc, stat, qb, po_s, po_r,
    st_s, st_r, tot_s, tot_r, in_s, in_r, pref, qc_scr, ol_scr,
    pbuf, prx,
    lsem, a_send, a_recv, r_send, r_recv,
    gy_send, gy_recv, gz_send, gz_recv,
    po_send, po_recv,
    st_send, st_recv, tot_send, tot_recv, in_send, in_recv,
    p_send, p_recv,
):
    p = lax.axis_index("sp")
    x = lax.axis_index("fs")
    t = lax.axis_index("tp")
    z = p // ny
    y = p % ny
    t_other = 1 - t
    xl = (x + 3) % 4
    xr = (x + 1) % 4
    xo = (x + 2) % 4
    slice_rows = DV // ny

    open_scope = []

    def phase(name):
        if open_scope:
            open_scope.pop().__exit__(None, None, None)
        if name:
            scope = jax.named_scope(name)
            scope.__enter__()
            open_scope.append(scope)

    phase("start")
    weights = (wq, wk, wv, wrq, wrf, wri)
    tok_copy = pltpu.make_async_copy(tok_hbm, tok, lsem.at[0])
    tok_copy.start()
    w_copies = [
        pltpu.make_async_copy(w, wcat.at[pl.ds(i * DK, DK)], lsem.at[1 + i]) for i, w in enumerate(weights)
    ]
    for c in w_copies:
        c.start()
    wo_copies = [
        pltpu.make_async_copy(wa_hbm, wo.at[0], lsem.at[7]),
        pltpu.make_async_copy(wr_hbm, wo.at[1], lsem.at[8]),
    ]
    for c in wo_copies:
        c.start()

    barrier = pltpu.get_barrier_semaphore()

    def greet(dev):
        pl.semaphore_signal(barrier, inc=1, device_id=dev, device_id_type=MESH)

    greet({"tp": t_other})
    for d in range(1, 4):
        greet({"fs": (x + d) % 4})
    for d in range(1, ny):
        greet({"sp": z * ny + (y + d) % ny})
    for d in range(1, nz):
        greet({"sp": ((z + d) % nz) * ny + y})

    def remote(src, dst, ssem, rsem, dev):
        return pltpu.make_async_remote_copy(
            src_ref=src, dst_ref=dst, send_sem=ssem, recv_sem=rsem, device_id=dev, device_id_type=MESH
        )

    def piece(f, tt, pc):
        return nrm.at[f, pl.ds(pl.multiple_of(tt * 64 + pc * 32, 32), 32)]

    def a_sem(f, tt, pc):
        return a_recv.at[f, tt * 2 + pc]

    def normalise(tt, pc):
        rows = pl.ds(pl.multiple_of(tt * 64 + pc * 32, 32), 32)
        nrm[x, rows, :] = norm_rows(tok[rows, :].astype(F32), gain_ref[...]).astype(BF16)

    acc[...] = jnp.zeros_like(acc)
    stat[...] = jnp.full(stat.shape, NEG, F32)
    tok_copy.wait()
    normalise(t, 0)
    normalise(t, 1)
    phase("entry_barrier")
    pl.semaphore_wait(barrier, 1 + 3 + (ny - 1) + (nz - 1))

    a_list = []

    def a_start(k, f, pc, dev):
        c = remote(piece(f, t, pc), piece(f, t, pc), a_send.at[k], a_sem(f, t, pc), dev)
        c.start()
        a_list.append(c)

    def a_wait(f, tt, pc):
        remote(piece(f, tt, pc), piece(f, tt, pc), a_send.at[0], a_sem(f, tt, pc), {"fs": xr}).wait_recv()

    phase("x_own")
    a_start(0, x, 0, {"fs": xr})
    a_start(1, x, 1, {"fs": xl})
    a_start(2, x, 1, {"fs": xr})
    a_start(3, x, 0, {"fs": xl})
    normalise(t_other, 0)
    normalise(t_other, 1)
    for i in range(6):
        w_copies[i].wait()

    def project(rows):
        return dot_nt(rows, wcat[...]).astype(BF16)

    own = project(nrm[x])
    res[x] = own[:, :FIRST]
    res2[x] = own[:, FIRST:]
    phase("x_forward")
    a_wait(xl, t, 0)
    a_start(4, xl, 0, {"fs": xr})
    a_start(5, xl, 0, {"tp": t_other})
    a_wait(xr, t, 1)
    a_start(6, xr, 1, {"fs": xl})
    a_start(7, xr, 1, {"tp": t_other})
    a_wait(xl, t, 1)
    a_start(8, xl, 1, {"tp": t_other})
    a_wait(xr, t, 0)
    a_start(9, xr, 0, {"tp": t_other})

    r_list = []

    def answer(k, f):
        for j, (out, into) in enumerate(((rsend, res), (rsend2, res2))):
            c = remote(out.at[k], into.at[x], r_send.at[k, j], r_recv.at[x, j], {"fs": f})
            c.start()
            r_list.append(c)

    phase("x_near")
    for f in (xl, xr):
        a_wait(f, t_other, 0)
        a_wait(f, t_other, 1)
    near = project(jnp.concatenate([nrm[xl], nrm[xr]], axis=0))
    for k in (0, 1):
        rsend[k] = near[k * ROWS:(k + 1) * ROWS, :FIRST]
        rsend2[k] = near[k * ROWS:(k + 1) * ROWS, FIRST:]
    answer(0, xl)
    answer(1, xr)
    phase("x_far")
    a_wait(xo, t, 0)
    a_start(10, xo, 0, {"tp": t_other})
    a_wait(xo, t, 1)
    a_start(11, xo, 1, {"tp": t_other})
    a_wait(xo, t_other, 0)
    a_wait(xo, t_other, 1)
    far = project(nrm[xo])
    rsend[2] = far[:, :FIRST]
    rsend2[2] = far[:, FIRST:]
    answer(2, xo)
    phase("x_answers")
    for f in (xl, xr, xo):
        remote(res.at[f], res.at[f], r_send.at[0, 0], r_recv.at[f, 0], {"fs": xr}).wait_recv()

    phase("tiles")
    def tile(kind, h):
        lo, ref = (kind * DK, res) if kind * DK < FIRST else (kind * DK - FIRST, res2)
        return jnp.concatenate([ref[2 * h, :, lo:lo + DK], ref[2 * h + 1, :, lo:lo + DK]], axis=1)

    def value_t(h):
        return tile(2, h).astype(F32).T.astype(BF16)

    scale_q = jnp.asarray(DK ** (-0.5), BF16)
    gy[0, 0] = (tile(0, 0) * scale_q).astype(F32).T.astype(BF16)
    gy[0, 1] = tile(1, 1)
    gy[0, 2] = value_t(1)
    gz[0, 0] = (tile(0, 1) * scale_q).astype(F32).T.astype(BF16)
    gz[0, 1] = tile(1, 0)
    gz[0, 2] = value_t(0)

    def y_dev(yy):
        return {"sp": z * ny + yy}

    def z_dev(zz):
        return {"sp": zz * ny + y}

    g_list = []

    def pass_on(hop):
        for k in range(3):
            for buf, sent, got, me, size, dev in (
                (gy, gy_send, gy_recv, y, ny, y_dev), (gz, gz_send, gz_recv, z, nz, z_dev)
            ):
                for side, way in enumerate((1, -1)):
                    def carried(h):
                        return 2 * h < size or (2 * h == size and (k % 2 == 0) == (way == 1))

                    here = (-way * hop) % size
                    there = (-way * (hop + 1)) % size
                    dev_next = dev((me + size + way) % size)
                    if hop > 0 and carried(hop):
                        remote(buf.at[here, k], buf.at[here, k], sent.at[0, 0, 0], got.at[here, k], dev_next).wait_recv()
                    if carried(hop + 1):
                        c = remote(buf.at[here, k], buf.at[there, k], sent.at[side, hop, k], got.at[there, k], dev_next)
                        c.start()
                        g_list.append(c)

    pass_on(0)

    phase("rec_local")
    for f in (xl, xr, xo):
        remote(res2.at[f], res2.at[f], r_send.at[0, 1], r_recv.at[f, 1], {"fs": xr}).wait_recv()
    row = lax.broadcasted_iota(jnp.int32, (ROWS, ROWS), 0)
    col = lax.broadcasted_iota(jnp.int32, (ROWS, ROWS), 1)
    tril = jnp.where(row >= col, 1.0, 0.0).astype(F32)
    rates = []
    scale_col = jnp.broadcast_to(scale_ref[...], (ROWS, ROWS)).T
    for h in range(2):
        rq = tile(3, h).astype(F32)
        rf = tile(4, h).astype(F32)
        ri = tile(5, h)
        edge = lb_ref[h:h + 1, :]
        forget = edge + (1.0 - edge) * jax.nn.sigmoid(rf)
        g = scale_col * jnp.log(forget)
        kk = 1.0 - jnp.exp(g)
        cum = lax.dot_general(
            tril, g, (((1,), (0,)), ((), ())), precision=lax.Precision.HIGHEST, preferred_element_type=F32
        )
        scores = jnp.where(row == col, jnp.sum(rq * kk, axis=-1, keepdims=True), 0.0)
        c8 = cum.reshape(ROWS // 8, 8, DV)
        r8 = lax.broadcasted_iota(jnp.int32, (ROWS // 8, 8, DV), 1)
        for b in (64, 32, 16, 8, 4, 2, 1):
            if b >= 8:
                c3 = cum.reshape(ROWS // (2 * b), 2 * b, DV)
                diff = (c3 - c3[:, b - 1:b, :]).reshape(ROWS, DV)
            else:
                mid = c8[:, b - 1:b, :]
                for first in range(2 * b, 8, 2 * b):
                    mid = jnp.where(r8 >= first, c8[:, first + b - 1:first + b, :], mid)
                diff = (c8 - mid).reshape(ROWS, DV)
            upper = (row & (2 * b - 1)) >= b
            decay = jnp.exp(jnp.where(upper, diff, -diff))
            late = jnp.where(upper, rq * decay, 0.0).astype(BF16)
            early = jnp.where(upper, 0.0, kk * decay).astype(BF16)
            level = dot_nt(late, early)
            scores = scores + jnp.where((row ^ col) < 2 * b, level, 0.0)
        ol_scr[h] = dot_nn(scores.astype(BF16), ri)
        last = cum[ROWS - 1:ROWS, :]
        key_end = (kk * jnp.exp(last - cum)).astype(BF16)
        state_t = dot_nn(ri.astype(F32).T.astype(BF16), key_end)
        qc_scr[h] = (rq * jnp.exp(cum)).astype(BF16)
        st_s[:, h * slice_rows:(h + 1) * slice_rows, :] = state_t.reshape(ny, slice_rows, DV).astype(BF16)
        rates.append(jnp.exp(last))
    packed = pack_rates(*rates)
    for k in range(ny):
        st_s[k, 2 * slice_rows:, :] = packed
    def state_send():
        st_r[y] = st_s[y]
        for d in range(1, ny):
            yy = (y + d) % ny
            c = remote(st_s.at[yy], st_r.at[y], st_send.at[d], st_recv.at[y], y_dev(yy))
            c.start()
            g_list.append(c)

    half = slice_rows

    def step_of(ref):
        d0, d1 = unpack_rates(ref[2 * half:, :])
        return d0, ref[0:half, :].astype(F32), d1, ref[half:2 * half, :].astype(F32)

    def state_prefix():
        phase("rec_prefix")
        for d in range(1, ny):
            yy = (y + d) % ny
            remote(st_r.at[yy], st_r.at[yy], st_send.at[0], st_recv.at[yy], y_dev(yy)).wait_recv()

        s0 = s1 = jnp.zeros((half, DV), F32)
        c0 = c1 = jnp.ones((1, DV), F32)
        for k in range(ny):
            pref[k, 0:half, :] = s0
            pref[k, half:2 * half, :] = s1
            pref[k, 2 * half:2 * half + 8, :] = jnp.broadcast_to(c0, (8, DV))
            pref[k, 2 * half + 8:2 * half + 16, :] = jnp.broadcast_to(c1, (8, DV))
            d0, a0, d1, a1 = step_of(st_r.at[k])
            s0, s1, c0, c1 = d0 * s0 + a0, d1 * s1 + a1, c0 * d0, c1 * d1
        tot_s[0:half, :] = s0.astype(BF16)
        tot_s[half:2 * half, :] = s1.astype(BF16)
        tot_s[2 * half:, :] = pack_rates(c0, c1)
        for d in range(1, nz):
            zz = (z + d) % nz
            c = remote(tot_s, tot_r.at[z], tot_send.at[d], tot_recv.at[z], z_dev(zz))
            c.start()
            g_list.append(c)

    def state_entry():
        phase("rec_totals")
        for d in range(1, nz):
            zz = (z + d) % nz
            remote(tot_r.at[zz], tot_r.at[zz], tot_send.at[0], tot_recv.at[zz], z_dev(zz)).wait_recv()

        def fold(k, carry):
            d0, a0, d1, a1 = step_of(tot_r.at[k])
            return (d0 * carry[0] + a0, d1 * carry[1] + a1)

        entry = lax.fori_loop(0, z, fold, (jnp.zeros((half, DV), F32), jnp.zeros((half, DV), F32)))
        for k in range(ny):
            for h in range(2):
                d = pref[k, 2 * half + 8 * h:2 * half + 8 * h + 1, :]
                in_s[k, h] = (d * entry[h] + pref[k, h * half:(h + 1) * half, :]).astype(BF16)
        in_r[y] = in_s[y]
        for d in range(1, ny):
            yy = (y + d) % ny
            c = remote(in_s.at[yy], in_r.at[y], in_send.at[d], in_recv.at[y], y_dev(yy))
            c.start()
            g_list.append(c)

    channel = lax.broadcasted_iota(jnp.int32, (ROWS, DV), 0)
    below = (
        lax.broadcasted_iota(jnp.int32, (ROWS, 2 * ROWS), 0)
        <= (lax.broadcasted_iota(jnp.int32, (ROWS, 2 * ROWS), 1) & (ROWS - 1))
    )

    def seen(head, off):
        if off % nz == 0:
            return None
        other = (z + off % nz) % nz
        return other < z if head == 0 else other > z

    def when(condition, body):
        if condition is None:
            body()
        else:
            pl.when(condition)(body)

    def ring(hop, size):
        if hop == 0:
            return [0]
        if 2 * hop < size:
            return [hop, -hop]
        return [hop] if 2 * hop == size else []

    def within(hop, size):
        return [o for h in range(hop + 1) for o in ring(h, size)]

    def arrival(off, size):
        return [o % size for o in within(size, size)].index(off % size)

    def sides(head):
        return (gy, gz, ny, nz) if head == 0 else (gz, gy, nz, ny)

    def keep_queries(head, off):
        q_buf, _, q_size, _ = sides(head)
        queries = q_buf[off % q_size, 0]
        zero = jnp.zeros_like(queries)
        at = arrival(off, q_size) * 2 * ROWS
        qb[head, :, at:at + ROWS] = jnp.where(channel < DK, queries, zero)
        qb[head, :, at + ROWS:at + 2 * ROWS] = jnp.where(channel < DK, zero, queries)

    def hidden(head, q_off, k_off):
        _, _, q_size, k_size = sides(head)
        if head == 0:
            if k_off % nz == 0:
                return y > (y + q_off % ny) % ny
            return (z + k_off % nz) % nz > z
        if q_off % nz == 0:
            return (y + k_off % ny) % ny > y
        return (z + q_off % nz) % nz < z

    def attend(head, q_offs, k_offs, checked=True):
        _, kv_buf, q_size, k_size = sides(head)
        if not q_offs or not k_offs:
            return
        lo = arrival(q_offs[0], q_size) * 2 * ROWS
        hi = lo + len(q_offs) * 2 * ROWS
        slots = [o % k_size for o in k_offs]
        s = dot_nn(jnp.concatenate([kv_buf[i, 1] for i in slots], axis=0), qb[head, :, lo:hi])
        parts = []
        for i, k_off in enumerate(k_offs):
            part = s[i * ROWS:(i + 1) * ROWS]
            blocks = []
            for j, q_off in enumerate(q_offs):
                block = part[:, j * 2 * ROWS:(j + 1) * 2 * ROWS]
                if q_off % q_size == 0 and k_off % k_size == 0:
                    block = jnp.where(below, block, NEG)
                elif checked or (k_off if head == 0 else q_off) % nz == 0:
                    block = block + jnp.where(hidden(head, q_off, k_off), NEG, 0.0).astype(F32)
                blocks.append(block)
            parts.append(jnp.concatenate(blocks, axis=1))
        width = hi - lo
        best = jnp.max(functools.reduce(jnp.maximum, parts).reshape(ROWS // 8, 8, width), axis=0)
        top = stat[head, 0:1, lo:hi]
        now = jnp.maximum(top, jnp.max(best, axis=0, keepdims=True))
        es = [jnp.exp(part - now) for part in parts]
        summed = functools.reduce(jnp.add, [jnp.sum(e.reshape(ROWS // 8, 8, width), axis=0) for e in es])
        new = dot_nn(
            jnp.concatenate([kv_buf[i, 2] for i in slots], axis=1),
            jnp.concatenate([e.astype(BF16) for e in es], axis=0),
        )
        keep = jnp.exp(top - now)
        stat[head, 0:1, lo:hi] = now
        stat[head, 1:2, lo:hi] = keep * stat[head, 1:2, lo:hi] + jnp.sum(summed, axis=0, keepdims=True)
        acc[head, :, lo:hi] = keep * acc[head, :, lo:hi] + new

    def early(hop):
        queries, keys = within(hop, ny), within(hop, nz)
        for k in keys:
            when(seen(0, k), lambda k=k: attend(0, queries, [k], False))
        queries, keys = within(hop, nz), within(hop, ny)
        for q in queries:
            when(seen(1, q), lambda q=q: attend(1, [q], keys, False))

    def late_queries(hop):
        keys = within(hop, nz)
        attend(0, ring(hop, ny), [k for k in keys if k <= 0])
        rest = [k for k in keys if k > 0]
        if rest and ring(hop, ny):
            pl.when(z + max(rest) >= nz)(lambda: attend(0, ring(hop, ny), rest))
        for q in ring(hop, nz):
            when(seen(1, q), lambda q=q: attend(1, [q], within(hop, ny), False))

    def late_keys(hop):
        for k in ring(hop, nz):
            when(seen(0, k), lambda k=k: attend(0, within(hop - 1, ny), [k], False))
        attend(1, within(hop - 1, nz), ring(hop, ny))

    rings = ((0, y, ny, y_dev), (1, z, nz, z_dev))

    def load_own(head, off, size):
        lo = arrival(off, size) * 2 * ROWS
        hi = lo + 2 * ROWS
        return stat[head, 0:1, lo:hi], stat[head, 1:2, lo:hi], acc[head, :, lo:hi]

    def combine(one, message):
        top, total, num = one
        t0, l0, t1, l1 = unpack_stats(message[2 * DV:, :])
        new_top = jnp.concatenate([t0, t1], axis=1)
        now = jnp.maximum(top, new_top)
        keep = jnp.exp(top - now)
        weight = jnp.exp(new_top - now)
        new_num = jnp.concatenate([message[0:DV, :].astype(F32), message[DV:2 * DV, :].astype(F32)], axis=1)
        total = keep * total + weight * jnp.concatenate([l0, l1], axis=1)
        return now, total, keep * num + weight * new_num

    def send_partial(head, side, dist, value, me, size, dev):
        way = -1 if side == 0 else 1
        top, total, num = value
        out = po_s.at[head, side, dist]
        out[0:DV, :] = num[:, :ROWS].astype(BF16)
        out[DV:2 * DV, :] = num[:, ROWS:].astype(BF16)
        out[2 * DV:, :] = pack_stats([top[:, :ROWS], total[:, :ROWS], top[:, ROWS:], total[:, ROWS:]])
        step = dist if dist <= 2 else 1
        c = remote(
            out, po_r.at[head, side, dist], po_send.at[head, side, dist], po_recv.at[head, side, dist],
            dev((me + size + way * step) % size),
        )
        c.start()
        g_list.append(c)

    def await_partial(head, side, dist, dev, me):
        remote(
            po_r.at[head, side, dist], po_r.at[head, side, dist],
            po_send.at[head, side, dist], po_recv.at[head, side, dist], dev(me),
        ).wait_recv()
        return po_r.at[head, side, dist]

    def reach(side, size):
        return size // 2 if side == 0 else (size - 1) // 2

    def own_part(head, side, dist, me, size, dev):
        way = -1 if side == 0 else 1
        send_partial(head, side, dist, load_own(head, way * dist, size), me, size, dev)

    def passing(head, side, dist, me, size, dev):
        way = -1 if side == 0 else 1
        got = await_partial(head, side, dist + 1, dev, me)
        send_partial(head, side, dist, combine(load_own(head, way * dist, size), got), me, size, dev)

    last_hop = max(ny, nz) // 2
    def keep_arrived(hop):
        for head, size in ((0, ny), (1, nz)):
            for q in ring(hop, size):
                keep_queries(head, q)

    def send_far():
        for head, me, size, dev in rings:
            if size // 2 == last_hop:
                own_part(head, 0, reach(0, size), me, size, dev)

    keep_arrived(0)
    first_round = min(1, last_hop - 1)
    if first_round == 0:
        early(0)
    for hop in range(1, last_hop + 1):
        phase("gather_hop" + str(hop))
        pass_on(hop)
        if hop == min(2, last_hop):
            state_send()
        keep_arrived(hop)
        if hop == first_round:
            phase("early")
            early(hop)
        elif hop > first_round:
            phase("late_queries" + str(hop))
            late_queries(hop)
            if hop == last_hop:
                send_far()
            phase("late_keys" + str(hop))
            late_keys(hop)
            if hop == min(3, last_hop):
                state_prefix()
    phase("partials")
    for dist in (4, 3, 2, 1):
        for head, me, size, dev in rings:
            for side in (1, 0):
                unsent = side == 1 or size // 2 < last_hop
                if dist == reach(side, size) and unsent or dist == 1 and reach(side, size) > 1:
                    own_part(head, side, dist, me, size, dev)
    phase("pass_far")
    for dist in (3, 2):
        if dist == 2:
            state_entry()
            phase("pass_near")
        for head, me, size, dev in rings:
            for side in (1, 0):
                if dist + 1 <= reach(side, size) and dist + 1 > 2:
                    passing(head, side, dist, me, size, dev)
                elif dist == 2 and dist < reach(side, size):
                    own_part(head, side, dist, me, size, dev)

    def finish(head, value):
        top, total, num = value
        att = num[:, :ROWS] / total[:, :ROWS] - lam_ref[head] * num[:, ROWS:] / total[:, ROWS:]
        att = att * lax.rsqrt(jnp.mean(att * att, axis=0, keepdims=True) + EPS)
        lws_ref[head:head + 1, :] = top[:, :ROWS] + jnp.log(total[:, :ROWS])
        return (att.T * attg_ref[...] * 0.8).astype(BF16)

    phase("merge_own")
    att = []
    for head, me, size, dev in rings:
        value = load_own(head, 0, size)
        for dist in (1, 2):
            for side in (1, 0):
                if dist <= reach(side, size):
                    value = combine(value, await_partial(head, side, dist, dev, me))
        att.append(finish(head, value))
    att_rows = jnp.concatenate(att, axis=1)

    phase("rec_result")
    for d in range(1, ny):
        yy = (y + d) % ny
        remote(in_r.at[yy], in_r.at[yy], in_send.at[0], in_recv.at[yy], y_dev(yy)).wait_recv()
    rec = []
    for h in range(2):
        o = ol_scr[h] + dot_nt(qc_scr[h], in_r[:, h].reshape(DV, DV))
        rec.append(norm_rows(o, recg_ref[...]).astype(BF16))
    rec_rows = jnp.concatenate(rec, axis=1)

    phase("project_out")
    for c in wo_copies:
        c.wait()
    width = wo.shape[2] // PARTS
    p_list = []
    for k in range(PARTS):
        cols = slice(k * width, (k + 1) * width)
        part = dot_nn(att_rows, wo[0, :, cols]) + dot_nn(rec_rows, wo[1, :, cols])
        pbuf[k] = part.astype(BF16)
        c = remote(pbuf.at[k], prx.at[k], p_send.at[k], p_recv.at[k], {"tp": t_other})
        c.start()
        p_list.append(c)
    for k in range(PARTS):
        p_list[k].wait_recv()
        out_ref[:, k * width:(k + 1) * width] = (pbuf[k].astype(F32) + prx[k].astype(F32)).astype(BF16)

    phase("drain")
    for c in a_list + r_list + g_list + p_list:
        c.wait_send()
    phase(None)


def hand_over(mixed_ref, log_ref, mixed_out, log_out):
    mixed_out[...] = mixed_ref[...]
    log_out[...] = log_ref[...]


def on_device(nz, ny, tokens, in_gain, wq, wk, wv, wrq, wrf, wri, lam, lb, scale, attg, recg, wa, wr):
    d = tokens.shape[1]
    out_cols = wa.shape[1]
    any_spec = pl.BlockSpec(memory_space=pl.ANY)
    vmem = pl.BlockSpec(memory_space=pltpu.VMEM)
    smem = pl.BlockSpec(memory_space=pltpu.SMEM)
    slice_rows = DV // ny
    st_rows = 2 * slice_rows + 16
    dma = pltpu.SemaphoreType.DMA
    scratch = [
        pltpu.VMEM((ROWS, d), BF16),
        pltpu.VMEM((COLS, d), BF16),
        pltpu.VMEM((2, wa.shape[0], out_cols), BF16),
        pltpu.VMEM((FS, ROWS, d), BF16),
        pltpu.VMEM((FS, ROWS, FIRST), BF16),
        pltpu.VMEM((FS, ROWS, COLS - FIRST), BF16),
        pltpu.VMEM((3, ROWS, FIRST), BF16),
        pltpu.VMEM((3, ROWS, COLS - FIRST), BF16),
        pltpu.VMEM((ny, 3, ROWS, DV), BF16),
        pltpu.VMEM((nz, 3, ROWS, DV), BF16),
        pltpu.VMEM((2, DV, max(ny, nz) * 2 * ROWS), F32),
        pltpu.VMEM((2, 8, max(ny, nz) * 2 * ROWS), F32),
        pltpu.VMEM((2, DV, max(ny, nz) * 2 * ROWS), BF16),
        pltpu.VMEM((2, 2, 5, 2 * DV + 16, ROWS), BF16),
        pltpu.VMEM((2, 2, 5, 2 * DV + 16, ROWS), BF16),
        pltpu.VMEM((ny, st_rows, DV), BF16),
        pltpu.VMEM((ny, st_rows, DV), BF16),
        pltpu.VMEM((st_rows, DV), BF16),
        pltpu.VMEM((nz, st_rows, DV), BF16),
        pltpu.VMEM((ny, 2, slice_rows, DV), BF16),
        pltpu.VMEM((ny, 2, slice_rows, DV), BF16),
        pltpu.VMEM((ny, st_rows, DV), F32),
        pltpu.VMEM((2, ROWS, DV), BF16),
        pltpu.VMEM((2, ROWS, DV), F32),
        pltpu.VMEM((PARTS, ROWS, out_cols // PARTS), BF16),
        pltpu.VMEM((PARTS, ROWS, out_cols // PARTS), BF16),
        dma((9,)), dma((12,)), dma((FS, 4)), dma((3, 2)), dma((FS, 2)),
        dma((2, ny // 2 + 1, 3)), dma((ny, 3)), dma((2, nz // 2 + 1, 3)), dma((nz, 3)),
        dma((2, 2, 5)), dma((2, 2, 5)),
        dma((ny,)), dma((ny,)), dma((nz,)), dma((nz,)), dma((ny,)), dma((ny,)),
        dma((PARTS,)), dma((PARTS,)),
    ]
    mixed, log_sum = pl.pallas_call(
        functools.partial(kernel_body, nz, ny),
        out_shape=(
            jax.ShapeDtypeStruct((ROWS, out_cols), BF16),
            jax.ShapeDtypeStruct((2, ROWS), F32),
        ),
        in_specs=[any_spec, vmem] + [any_spec] * 6 + [smem, vmem, vmem, vmem, vmem, any_spec, any_spec],
        out_specs=(vmem, vmem),
        scratch_shapes=scratch,
        compiler_params=pltpu.CompilerParams(
            collective_id=0, has_side_effects=True, vmem_limit_bytes=56 * 1024 * 1024
        ),
    )(
        tokens, in_gain.reshape(1, d), wq.T, wk.T, wv.T, wrq.T, wrf.T, wri.T, lam, lb,
        scale.reshape(1, ROWS), attg.reshape(1, DV), recg.reshape(1, DV), wa, wr,
    )
    return pl.pallas_call(
        hand_over,
        out_shape=(
            jax.ShapeDtypeStruct((ROWS, out_cols), BF16),
            jax.ShapeDtypeStruct((2, ROWS), F32),
        ),
        in_specs=[vmem, vmem],
        out_specs=(vmem, vmem),
    )(mixed, log_sum)


def plane_of(size):
    nz = 1
    while nz * nz < size:
        nz *= 2
    return nz, size // nz


def solution(mesh):
    nz, ny = plane_of(mesh.shape["sp"])
    col_split = P(None, ("tp", "fs"))
    placed = (
        P(("fs", "sp"), None), P(),
        col_split, col_split, col_split, col_split, col_split, col_split,
        P("tp"), P("tp", None), P(("fs", "sp")), P(), P(),
        P("tp", None), P("tp", None),
    )
    return jax.shard_map(
        functools.partial(on_device, nz, ny),
        mesh=mesh,
        in_specs=placed,
        out_specs=(P(("fs", "sp"), None), P("tp", ("fs", "sp"))),
        check_vma=False,
    )
```

time: 75.9 us -> 70.8 us (0.933)
  Pallas kernels: 75.1 us -> 69.7 us
    pallas_call x1, Pallas kernels: 73.2 us -> 67.8 us  [on_device(): pl.pallas_call(functools.partial(kernel_body, nz, ny), out_shape=(jax.Sha...]
where the time goes in v3:
time: 70.8 us; the launch traced here: 70.3 us
  Pallas kernels  69.7 us (98%)
    pallas_call x1, Pallas kernels, on_device(): pl.pallas_call(functools.partial(kernel_body, nz, ny), out_shape=(jax.Sha...  67.8 us
    pallas_call x1, Pallas kernels, on_device(): pl.pallas_call(hand_over, out_shape=(jax.ShapeDtypeStruct((ROWS, out_cols...  1.87 us

profile of v3, /device:TPU:1, one launch (start us, length us, event | category | flops | bytes accessed | tf_op | source)
XLA Modules:
  0.0 70.3 jit_solution(10781587615912022873)
XLA Ops:
  0.6 67.8 %shard_map.158 = (bf16[128,2048]{1,0:T(8,128)(2,1)}, f32[2,128]{1,0:T(2,128)}) custom-call(bf16[128,2048]{1,0:T(8,128)(2,1)} %tok_hbm.1, f32[1,2048]{1,0:T(1,128)} %bitcast.16, bf16[64,2048]{1,0:T(8,128)(2,1)} %bitcast.10, bf16[64,2048]{1,0:T(8,128)(2,1)} %bitcast.11, bf16[64,2048]{1,0:T(8,128)(2,1)} %bitcast.12, bf16[64,2048]{1,0:T(8,128)(2,1)} %bitcast.13, ...), custom_call_target="tpu_custom_call" | custom-call | tf_op jit(solution)/shard_map/pallas_call | solution.py:687
  68.5 1.9 %shard_map.159 = (bf16[128,2048]{1,0:T(8,128)(2,1)}, f32[2,128]{1,0:T(2,128)}) custom-call(bf16[128,2048]{1,0:T(8,128)(2,1)} %get-tuple-element.4.mixed_ref, f32[2,128]{1,0:T(2,128)} %get-tuple-element.5.log_ref), custom_call_target="tpu_custom_call" | custom-call | tf_op jit(solution)/shard_map/pallas_call | solution.py:703

commit v4 on v3

--- a/solution.py
+++ b/solution.py
@@ -53,9 +53,9 @@
     return tile.astype(BF16)
 
 
-def unpack_stats(packed):
+def unpack_stats(packed, count=4):
     wide = packed.astype(F32)
-    return [wide[3 * i:3 * i + 1] + wide[3 * i + 1:3 * i + 2] + wide[3 * i + 2:3 * i + 3] for i in range(4)]
+    return [wide[3 * i:3 * i + 1] + wide[3 * i + 1:3 * i + 2] + wide[3 * i + 2:3 * i + 3] for i in range(count)]
 
 
 def norm_rows(values, gain):
@@ -69,12 +69,12 @@
     wa_hbm, wr_hbm,
     out_ref, lws_ref,
     tok, wcat, wo, nrm, res, res2, rsend, rsend2,
-    gy, gz, acc, stat, qb, po_s, po_r,
+    gy, gz, acc, stat, qb, po_s, po_r, pf_s, pf_r,
     st_s, st_r, tot_s, tot_r, in_s, in_r, pref, qc_scr, ol_scr,
     pbuf, prx,
     lsem, a_send, a_recv, r_send, r_recv,
     gy_send, gy_recv, gz_send, gz_recv,
-    po_send, po_recv,
+    po_send, po_recv, pf_send, pf_recv,
     st_send, st_recv, tot_send, tot_recv, in_send, in_recv,
     p_send, p_recv,
 ):
@@ -143,20 +143,15 @@
         rows = pl.ds(pl.multiple_of(tt * 64 + pc * 32, 32), 32)
         nrm[x, rows, :] = norm_rows(tok[rows, :].astype(F32), gain_ref[...]).astype(BF16)
 
-    acc[...] = jnp.zeros_like(acc)
-    stat[...] = jnp.full(stat.shape, NEG, F32)
     tok_copy.wait()
     normalise(t, 0)
     normalise(t, 1)
     phase("entry_barrier")
     pl.semaphore_wait(barrier, 1 + 3 + (ny - 1) + (nz - 1))
 
-    a_list = []
-
     def a_start(k, f, pc, dev):
-        c = remote(piece(f, t, pc), piece(f, t, pc), a_send.at[k], a_sem(f, t, pc), dev)
+        c = remote(piece(f, t, pc), piece(f, t, pc), a_send.at[0], a_sem(f, t, pc), dev)
         c.start()
-        a_list.append(c)
 
     def a_wait(f, tt, pc):
         remote(piece(f, tt, pc), piece(f, tt, pc), a_send.at[0], a_sem(f, tt, pc), {"fs": xr}).wait_recv()
@@ -174,6 +169,8 @@
     def project(rows):
         return dot_nt(rows, wcat[...]).astype(BF16)
 
+    acc[...] = jnp.zeros_like(acc)
+    stat[...] = jnp.full(stat.shape, NEG, F32)
     own = project(nrm[x])
     res[x] = own[:, :FIRST]
     res2[x] = own[:, FIRST:]
@@ -189,13 +186,9 @@
     a_wait(xr, t, 0)
     a_start(9, xr, 0, {"tp": t_other})
 
-    r_list = []
-
     def answer(k, f):
         for j, (out, into) in enumerate(((rsend, res), (rsend2, res2))):
-            c = remote(out.at[k], into.at[x], r_send.at[k, j], r_recv.at[x, j], {"fs": f})
-            c.start()
-            r_list.append(c)
+            remote(out.at[k], into.at[x], r_send.at[j], r_recv.at[j], {"fs": f}).start()
 
     phase("x_near")
     for f in (xl, xr):
@@ -219,8 +212,11 @@
     rsend2[2] = far[:, FIRST:]
     answer(2, xo)
     phase("x_answers")
-    for f in (xl, xr, xo):
-        remote(res.at[f], res.at[f], r_send.at[0, 0], r_recv.at[f, 0], {"fs": xr}).wait_recv()
+    def all_of(buf, count, send, recv):
+        part = buf.at[pl.ds(0, count)]
+        return remote(part, part, send, recv, {"tp": t_other})
+
+    all_of(res, 3, r_send.at[0], r_recv.at[0]).wait_recv()
 
     phase("tiles")
     def tile(kind, h):
@@ -244,14 +240,12 @@
     def z_dev(zz):
         return {"sp": zz * ny + y}
 
-    g_list = []
-
     def pass_on(hop):
         for k in range(3):
             for buf, sent, got, me, size, dev in (
                 (gy, gy_send, gy_recv, y, ny, y_dev), (gz, gz_send, gz_recv, z, nz, z_dev)
             ):
-                for side, way in enumerate((1, -1)):
+                for way in (1, -1):
                     def carried(h):
                         return 2 * h < size or (2 * h == size and (k % 2 == 0) == (way == 1))
 
@@ -259,17 +253,14 @@
                     there = (-way * (hop + 1)) % size
                     dev_next = dev((me + size + way) % size)
                     if hop > 0 and carried(hop):
-                        remote(buf.at[here, k], buf.at[here, k], sent.at[0, 0, 0], got.at[here, k], dev_next).wait_recv()
+                        remote(buf.at[here, k], buf.at[here, k], sent.at[0], got.at[here, k], dev_next).wait_recv()
                     if carried(hop + 1):
-                        c = remote(buf.at[here, k], buf.at[there, k], sent.at[side, hop, k], got.at[there, k], dev_next)
-                        c.start()
-                        g_list.append(c)
+                        remote(buf.at[here, k], buf.at[there, k], sent.at[0], got.at[there, k], dev_next).start()
 
     pass_on(0)
 
     phase("rec_local")
-    for f in (xl, xr, xo):
-        remote(res2.at[f], res2.at[f], r_send.at[0, 1], r_recv.at[f, 1], {"fs": xr}).wait_recv()
+    all_of(res2, 3, r_send.at[1], r_recv.at[1]).wait_recv()
     row = lax.broadcasted_iota(jnp.int32, (ROWS, ROWS), 0)
     col = lax.broadcasted_iota(jnp.int32, (ROWS, ROWS), 1)
     tril = jnp.where(row >= col, 1.0, 0.0).astype(F32)
@@ -318,9 +309,7 @@
         st_r[y] = st_s[y]
         for d in range(1, ny):
             yy = (y + d) % ny
-            c = remote(st_s.at[yy], st_r.at[y], st_send.at[d], st_recv.at[y], y_dev(yy))
-            c.start()
-            g_list.append(c)
+            remote(st_s.at[yy], st_r.at[y], st_send.at[0], st_recv.at[0], y_dev(yy)).start()
 
     half = slice_rows
 
@@ -330,9 +319,7 @@
 
     def state_prefix():
         phase("rec_prefix")
-        for d in range(1, ny):
-            yy = (y + d) % ny
-            remote(st_r.at[yy], st_r.at[yy], st_send.at[0], st_recv.at[yy], y_dev(yy)).wait_recv()
+        all_of(st_r, ny - 1, st_send.at[0], st_recv.at[0]).wait_recv()
 
         s0 = s1 = jnp.zeros((half, DV), F32)
         c0 = c1 = jnp.ones((1, DV), F32)
@@ -348,15 +335,11 @@
         tot_s[2 * half:, :] = pack_rates(c0, c1)
         for d in range(1, nz):
             zz = (z + d) % nz
-            c = remote(tot_s, tot_r.at[z], tot_send.at[d], tot_recv.at[z], z_dev(zz))
-            c.start()
-            g_list.append(c)
+            remote(tot_s, tot_r.at[z], tot_send.at[0], tot_recv.at[0], z_dev(zz)).start()
 
     def state_entry():
         phase("rec_totals")
-        for d in range(1, nz):
-            zz = (z + d) % nz
-            remote(tot_r.at[zz], tot_r.at[zz], tot_send.at[0], tot_recv.at[zz], z_dev(zz)).wait_recv()
+        all_of(tot_r, nz - 1, tot_send.at[0], tot_recv.at[0]).wait_recv()
 
         def fold(k, carry):
             d0, a0, d1, a1 = step_of(tot_r.at[k])
@@ -370,9 +353,7 @@
         in_r[y] = in_s[y]
         for d in range(1, ny):
             yy = (y + d) % ny
-            c = remote(in_s.at[yy], in_r.at[y], in_send.at[d], in_recv.at[y], y_dev(yy))
-            c.start()
-            g_list.append(c)
+            remote(in_s.at[yy], in_r.at[y], in_send.at[0], in_recv.at[0], y_dev(yy)).start()
 
     channel = lax.broadcasted_iota(jnp.int32, (ROWS, DV), 0)
     below = (
@@ -485,6 +466,36 @@
 
     rings = ((0, y, ny, y_dev), (1, z, nz, z_dev))
 
+    def reach(side, size):
+        return (size - 1) // 2 if side == 1 or size == 8 else size // 2
+
+    routes = [
+        (head, side, dist) for head, _, size, _ in rings for side in (0, 1) for dist in range(1, reach(side, size) + 1)
+    ]
+    halves = [(head, side) for head, _, size, _ in rings if size == 8 for side in (0, 1)]
+
+    def send_half(head, side, me, size, dev):
+        top, total, num = load_own(head, size // 2, size)
+        lanes = slice(side * ROWS, (side + 1) * ROWS)
+        at = halves.index((head, side))
+        pf_s[at, 0:DV, :] = num[:, lanes].astype(BF16)
+        pf_s[at, DV:, :] = pack_stats([top[:, lanes], total[:, lanes]])
+        hop = -2 if side == 0 else 2
+        remote(pf_s.at[at], pf_r.at[at], pf_send.at[0], pf_recv.at[at], dev((me + size + hop) % size)).start()
+
+    def combine_half(value, head, side, dev, me):
+        at = halves.index((head, side))
+        remote(pf_r.at[at], pf_r.at[at], pf_send.at[0], pf_recv.at[at], dev(me)).wait_recv()
+        lanes = slice(side * ROWS, (side + 1) * ROWS)
+        new_top, new_total = unpack_stats(pf_r[at, DV:, :], 2)
+        top, total, num = (v[:, lanes] for v in value)
+        now = jnp.maximum(top, new_top)
+        keep, weight = jnp.exp(top - now), jnp.exp(new_top - now)
+        merged = (now, keep * total + weight * new_total, keep * num + weight * pf_r[at, 0:DV, :].astype(F32))
+        rest = [v[:, (1 - side) * ROWS:(2 - side) * ROWS] for v in value]
+        pairs = zip(merged, rest) if side == 0 else zip(rest, merged)
+        return tuple(jnp.concatenate(pair, axis=1) for pair in pairs)
+
     def load_own(head, off, size):
         lo = arrival(off, size) * 2 * ROWS
         hi = lo + 2 * ROWS
@@ -504,27 +515,21 @@
     def send_partial(head, side, dist, value, me, size, dev):
         way = -1 if side == 0 else 1
         top, total, num = value
-        out = po_s.at[head, side, dist]
+        at = routes.index((head, side, dist))
+        out = po_s.at[at]
         out[0:DV, :] = num[:, :ROWS].astype(BF16)
         out[DV:2 * DV, :] = num[:, ROWS:].astype(BF16)
         out[2 * DV:, :] = pack_stats([top[:, :ROWS], total[:, :ROWS], top[:, ROWS:], total[:, ROWS:]])
-        step = dist if dist <= 2 else 1
-        c = remote(
-            out, po_r.at[head, side, dist], po_send.at[head, side, dist], po_recv.at[head, side, dist],
-            dev((me + size + way * step) % size),
-        )
-        c.start()
-        g_list.append(c)
+        step = min(dist, 2) if dist < 3 else 1
+        remote(
+            out, po_r.at[at], po_send.at[0], po_recv.at[at], dev((me + size + way * step) % size)
+        ).start()
 
     def await_partial(head, side, dist, dev, me):
-        remote(
-            po_r.at[head, side, dist], po_r.at[head, side, dist],
-            po_send.at[head, side, dist], po_recv.at[head, side, dist], dev(me),
-        ).wait_recv()
-        return po_r.at[head, side, dist]
-
-    def reach(side, size):
-        return size // 2 if side == 0 else (size - 1) // 2
+        at = routes.index((head, side, dist))
+        remote(po_r.at[at], po_r.at[at], po_send.at[0], po_recv.at[at], dev(me)).wait_recv()
+        return po_r.at[at]
+
 
     def own_part(head, side, dist, me, size, dev):
         way = -1 if side == 0 else 1
@@ -532,8 +537,12 @@
 
     def passing(head, side, dist, me, size, dev):
         way = -1 if side == 0 else 1
-        got = await_partial(head, side, dist + 1, dev, me)
-        send_partial(head, side, dist, combine(load_own(head, way * dist, size), got), me, size, dev)
+        value = load_own(head, way * dist, size)
+        if size == 8:
+            value = combine_half(value, head, side, dev, me)
+        for farther in range(dist + 1, reach(side, size) + 1):
+            value = combine(value, await_partial(head, side, farther, dev, me))
+        send_partial(head, side, dist, value, me, size, dev)
 
     last_hop = max(ny, nz) // 2
     def keep_arrived(hop):
@@ -543,7 +552,10 @@
 
     def send_far():
         for head, me, size, dev in rings:
-            if size // 2 == last_hop:
+            if size == 8:
+                for side in (0, 1):
+                    send_half(head, side, me, size, dev)
+            elif size // 2 == last_hop:
                 own_part(head, 0, reach(0, size), me, size, dev)
 
     keep_arrived(0)
@@ -569,23 +581,22 @@
             if hop == min(3, last_hop):
                 state_prefix()
     phase("partials")
-    for dist in (4, 3, 2, 1):
+    for dist in (3, 1):
         for head, me, size, dev in rings:
             for side in (1, 0):
-                unsent = side == 1 or size // 2 < last_hop
+                unsent = side == 1 or size // 2 < last_hop or size == 8
                 if dist == reach(side, size) and unsent or dist == 1 and reach(side, size) > 1:
                     own_part(head, side, dist, me, size, dev)
     phase("pass_far")
-    for dist in (3, 2):
-        if dist == 2:
+    for side in (1, 0):
+        for head, me, size, dev in rings:
+            if reach(side, size) > 2:
+                passing(head, side, 2, me, size, dev)
+            elif reach(side, size) == 2 and size // 2 < last_hop:
+                own_part(head, side, 2, me, size, dev)
+        if side == 1:
             state_entry()
             phase("pass_near")
-        for head, me, size, dev in rings:
-            for side in (1, 0):
-                if dist + 1 <= reach(side, size) and dist + 1 > 2:
-                    passing(head, side, dist, me, size, dev)
-                elif dist == 2 and dist < reach(side, size):
-                    own_part(head, side, dist, me, size, dev)
 
     def finish(head, value):
         top, total, num = value
@@ -606,9 +617,7 @@
     att_rows = jnp.concatenate(att, axis=1)
 
     phase("rec_result")
-    for d in range(1, ny):
-        yy = (y + d) % ny
-        remote(in_r.at[yy], in_r.at[yy], in_send.at[0], in_recv.at[yy], y_dev(yy)).wait_recv()
+    all_of(in_r, ny - 1, in_send.at[0], in_recv.at[0]).wait_recv()
     rec = []
     for h in range(2):
         o = ol_scr[h] + dot_nt(qc_scr[h], in_r[:, h].reshape(DV, DV))
@@ -624,7 +633,7 @@
         cols = slice(k * width, (k + 1) * width)
         part = dot_nn(att_rows, wo[0, :, cols]) + dot_nn(rec_rows, wo[1, :, cols])
         pbuf[k] = part.astype(BF16)
-        c = remote(pbuf.at[k], prx.at[k], p_send.at[k], p_recv.at[k], {"tp": t_other})
+        c = remote(pbuf.at[k], prx.at[k], p_send.at[0], p_recv.at[k], {"tp": t_other})
         c.start()
         p_list.append(c)
     for k in range(PARTS):
@@ -632,14 +641,15 @@
         out_ref[:, k * width:(k + 1) * width] = (pbuf[k].astype(F32) + prx[k].astype(F32)).astype(BF16)
 
     phase("drain")
-    for c in a_list + r_list + g_list + p_list:
-        c.wait_send()
+    for buf, count, sem in (
+        (nrm, 3, a_send.at[0]), (rsend, 3, r_send.at[0]), (rsend2, 3, r_send.at[1]),
+        (gy, ny - 1, gy_send.at[0]), (gz, nz - 1, gz_send.at[0]), (st_r, ny - 1, st_send.at[0]),
+        (tot_r, nz - 1, tot_send.at[0]), (in_r, ny - 1, in_send.at[0]), (po_s, len(routes), po_send.at[0]),
+        (pf_s, len(halves), pf_send.at[0]), (pbuf, PARTS, p_send.at[0]),
+    ):
+        if count:
+            all_of(buf, count, sem, sem).wait_send()
     phase(None)
-
-
-def hand_over(mixed_ref, log_ref, mixed_out, log_out):
-    mixed_out[...] = mixed_ref[...]
-    log_out[...] = log_ref[...]
 
 
 def on_device(nz, ny, tokens, in_gain, wq, wk, wv, wrq, wrf, wri, lam, lb, scale, attg, recg, wa, wr):
@@ -665,8 +675,10 @@
         pltpu.VMEM((2, DV, max(ny, nz) * 2 * ROWS), F32),
         pltpu.VMEM((2, 8, max(ny, nz) * 2 * ROWS), F32),
         pltpu.VMEM((2, DV, max(ny, nz) * 2 * ROWS), BF16),
-        pltpu.VMEM((2, 2, 5, 2 * DV + 16, ROWS), BF16),
-        pltpu.VMEM((2, 2, 5, 2 * DV + 16, ROWS), BF16),
+        pltpu.VMEM((12, 2 * DV + 16, ROWS), BF16),
+        pltpu.VMEM((12, 2 * DV + 16, ROWS), BF16),
+        pltpu.VMEM((4, DV + 16, ROWS), BF16),
+        pltpu.VMEM((4, DV + 16, ROWS), BF16),
         pltpu.VMEM((ny, st_rows, DV), BF16),
         pltpu.VMEM((ny, st_rows, DV), BF16),
         pltpu.VMEM((st_rows, DV), BF16),
@@ -678,18 +690,15 @@
         pltpu.VMEM((2, ROWS, DV), F32),
         pltpu.VMEM((PARTS, ROWS, out_cols // PARTS), BF16),
         pltpu.VMEM((PARTS, ROWS, out_cols // PARTS), BF16),
-        dma((9,)), dma((12,)), dma((FS, 4)), dma((3, 2)), dma((FS, 2)),
-        dma((2, ny // 2 + 1, 3)), dma((ny, 3)), dma((2, nz // 2 + 1, 3)), dma((nz, 3)),
-        dma((2, 2, 5)), dma((2, 2, 5)),
-        dma((ny,)), dma((ny,)), dma((nz,)), dma((nz,)), dma((ny,)), dma((ny,)),
-        dma((PARTS,)), dma((PARTS,)),
+        dma((9,)), dma((1,)), dma((FS, 4)), dma((2,)), dma((2,)),
+        dma((1,)), dma((ny, 3)), dma((1,)), dma((nz, 3)),
+        dma((1,)), dma((12,)), dma((1,)), dma((4,)),
+        dma((1,)), dma((1,)), dma((1,)), dma((1,)), dma((1,)), dma((1,)),
+        dma((1,)), dma((PARTS,)),
     ]
     mixed, log_sum = pl.pallas_call(
         functools.partial(kernel_body, nz, ny),
-        out_shape=(
-            jax.ShapeDtypeStruct((ROWS, out_cols), BF16),
-            jax.ShapeDtypeStruct((2, ROWS), F32),
-        ),
+        out_shape=(pltpu.VMEM((ROWS, out_cols), BF16), pltpu.VMEM((2, ROWS), F32)),
         in_specs=[any_spec, vmem] + [any_spec] * 6 + [smem, vmem, vmem, vmem, vmem, any_spec, any_spec],
         out_specs=(vmem, vmem),
         scratch_shapes=scratch,
@@ -700,15 +709,7 @@
         tokens, in_gain.reshape(1, d), wq.T, wk.T, wv.T, wrq.T, wrf.T, wri.T, lam, lb,
         scale.reshape(1, ROWS), attg.reshape(1, DV), recg.reshape(1, DV), wa, wr,
     )
-    return pl.pallas_call(
-        hand_over,
-        out_shape=(
-            jax.ShapeDtypeStruct((ROWS, out_cols), BF16),
-            jax.ShapeDtypeStruct((2, ROWS), F32),
-        ),
-        in_specs=[vmem, vmem],
-        out_specs=(vmem, vmem),
-    )(mixed, log_sum)
+    return mixed, log_sum
 
 
 def plane_of(size):

time: 70.8 us -> 68.3 us (0.965)
  Pallas kernels: 69.7 us -> 66.2 us
  local copies, waits for them, and re-layouts: 0 us -> 1.36 us
    pallas_call x2 -> x1, Pallas kernels: 69.7 us -> 66.2 us  [on_device(): pl.pallas_call(functools.partial(kernel_body, nz, ny), out_shape=(pltpu.V...]
    unnamed x0 -> x2, local copies, waits for them, and re-layouts: none -> 1.36 us
where the time goes in v4:
time: 68.3 us; the launch traced here: 68.2 us
  Pallas kernels  66.2 us (97%)
  local copies, waits for them, and re-layouts  1.36 us (2%)
    pallas_call x1, Pallas kernels, on_device(): pl.pallas_call(functools.partial(kernel_body, nz, ny), out_shape=(pltpu.V...  66.2 us

profile of v4, /device:TPU:1, one launch (start us, length us, event | category | flops | bytes accessed | tf_op | source)
XLA Modules:
  0.0 68.2 jit_solution(441391745415078049)
XLA Ops:
  0.6 66.2 %shard_map.158 = (bf16[128,2048]{1,0:T(8,128)(2,1)S(1)}, f32[2,128]{1,0:T(2,128)S(1)}) custom-call(bf16[128,2048]{1,0:T(8,128)(2,1)} %tok_hbm.1, f32[1,2048]{1,0:T(1,128)} %bitcast.16, bf16[64,2048]{1,0:T(8,128)(2,1)} %bitcast.10, bf16[64,2048]{1,0:T(8,128)(2,1)} %bitcast.11, bf16[64,2048]{1,0:T(8,128)(2,1)} %bitcast.12, bf16[64,2048]{1,0:T(8,128)(2,1)} %bitcast.13, ...), custom_call_target="tpu_custom_call" | custom-call | tf_op jit(solution)/shard_map/pallas_call | solution.py:699
  66.8 0.8 %copy.19 = bf16[128,2048]{1,0:T(8,128)(2,1)} copy(bf16[128,2048]{1,0:T(8,128)(2,1)S(1)} %get-tuple-element.2) | data formatting | bytes 1048576
  67.6 0.6 copy.20

commit v5 on v4

--- a/solution.py
+++ b/solution.py
@@ -71,7 +71,7 @@
     tok, wcat, wo, nrm, res, res2, rsend, rsend2,
     gy, gz, acc, stat, qb, po_s, po_r, pf_s, pf_r,
     st_s, st_r, tot_s, tot_r, in_s, in_r, pref, qc_scr, ol_scr,
-    pbuf, prx,
+    pbuf, prx, half_out,
     lsem, a_send, a_recv, r_send, r_recv,
     gy_send, gy_recv, gz_send, gz_recv,
     po_send, po_recv, pf_send, pf_recv,
@@ -452,7 +452,13 @@
 
     def late_queries(hop):
         keys = within(hop, nz)
-        attend(0, ring(hop, ny), [k for k in keys if k <= 0])
+        before = [k for k in keys if k <= 0]
+        close = [k for k in before if k >= -1]
+        if len(close) < len(before) and ring(hop, ny):
+            pl.when(z < 2)(lambda: attend(0, ring(hop, ny), close))
+            pl.when(z >= 2)(lambda: attend(0, ring(hop, ny), before))
+        else:
+            attend(0, ring(hop, ny), before)
         rest = [k for k in keys if k > 0]
         if rest and ring(hop, ny):
             pl.when(z + max(rest) >= nz)(lambda: attend(0, ring(hop, ny), rest))
@@ -462,7 +468,12 @@
     def late_keys(hop):
         for k in ring(hop, nz):
             when(seen(0, k), lambda k=k: attend(0, within(hop - 1, ny), [k], False))
-        attend(1, within(hop - 1, nz), ring(hop, ny))
+        queries, close = within(hop - 1, nz), within(1, nz)
+        if len(close) < len(queries) and ring(hop, ny):
+            pl.when(z >= nz - 2)(lambda: attend(1, close, ring(hop, ny)))
+            pl.when(z < nz - 2)(lambda: attend(1, queries, ring(hop, ny)))
+        else:
+            attend(1, queries, ring(hop, ny))
 
     rings = ((0, y, ny, y_dev), (1, z, nz, z_dev))
 
@@ -587,6 +598,7 @@
                 unsent = side == 1 or size // 2 < last_hop or size == 8
                 if dist == reach(side, size) and unsent or dist == 1 and reach(side, size) > 1:
                     own_part(head, side, dist, me, size, dev)
+    state_entry()
     phase("pass_far")
     for side in (1, 0):
         for head, me, size, dev in rings:
@@ -594,9 +606,6 @@
                 passing(head, side, 2, me, size, dev)
             elif reach(side, size) == 2 and size // 2 < last_hop:
                 own_part(head, side, 2, me, size, dev)
-        if side == 1:
-            state_entry()
-            phase("pass_near")
 
     def finish(head, value):
         top, total, num = value
@@ -604,17 +613,6 @@
         att = att * lax.rsqrt(jnp.mean(att * att, axis=0, keepdims=True) + EPS)
         lws_ref[head:head + 1, :] = top[:, :ROWS] + jnp.log(total[:, :ROWS])
         return (att.T * attg_ref[...] * 0.8).astype(BF16)
-
-    phase("merge_own")
-    att = []
-    for head, me, size, dev in rings:
-        value = load_own(head, 0, size)
-        for dist in (1, 2):
-            for side in (1, 0):
-                if dist <= reach(side, size):
-                    value = combine(value, await_partial(head, side, dist, dev, me))
-        att.append(finish(head, value))
-    att_rows = jnp.concatenate(att, axis=1)
 
     phase("rec_result")
     all_of(in_r, ny - 1, in_send.at[0], in_recv.at[0]).wait_recv()
@@ -624,14 +622,27 @@
         rec.append(norm_rows(o, recg_ref[...]).astype(BF16))
     rec_rows = jnp.concatenate(rec, axis=1)
 
-    phase("project_out")
     for c in wo_copies:
         c.wait()
     width = wo.shape[2] // PARTS
+    for k in range(PARTS):
+        half_out[k] = dot_nn(rec_rows, wo[1, :, k * width:(k + 1) * width])
+
+    phase("merge_own")
+    values = [load_own(head, 0, size) for head, _, size, _ in rings]
+    for dist in (1, 2):
+        for head, me, size, dev in rings:
+            for side in (1, 0):
+                if dist <= reach(side, size):
+                    values[head] = combine(values[head], await_partial(head, side, dist, dev, me))
+    att = [finish(head, values[head]) for head in (0, 1)]
+    att_rows = jnp.concatenate(att, axis=1)
+
+    phase("project_out")
     p_list = []
     for k in range(PARTS):
         cols = slice(k * width, (k + 1) * width)
-        part = dot_nn(att_rows, wo[0, :, cols]) + dot_nn(rec_rows, wo[1, :, cols])
+        part = dot_nn(att_rows, wo[0, :, cols]) + half_out[k]
         pbuf[k] = part.astype(BF16)
         c = remote(pbuf.at[k], prx.at[k], p_send.at[0], p_recv.at[k], {"tp": t_other})
         c.start()
@@ -690,6 +701,7 @@
         pltpu.VMEM((2, ROWS, DV), F32),
         pltpu.VMEM((PARTS, ROWS, out_cols // PARTS), BF16),
         pltpu.VMEM((PARTS, ROWS, out_cols // PARTS), BF16),
+        pltpu.VMEM((PARTS, ROWS, out_cols // PARTS), F32),
         dma((9,)), dma((1,)), dma((FS, 4)), dma((2,)), dma((2,)),
         dma((1,)), dma((ny, 3)), dma((1,)), dma((nz, 3)),
         dma((1,)), dma((12,)), dma((1,)), dma((4,)),

time: 68.3 us -> 67.1 us (0.982)
  Pallas kernels: 66.2 us -> 65 us
    pallas_call x1, Pallas kernels: 66.2 us -> 65 us  [on_device(): pl.pallas_call(functools.partial(kernel_body, nz, ny), out_shape=(pltpu.V...]
where the time goes in v5:
time: 67.1 us; the launch traced here: 67 us
  Pallas kernels  65 us (97%)
  local copies, waits for them, and re-layouts  1.36 us (2%)
    pallas_call x1, Pallas kernels, on_device(): pl.pallas_call(functools.partial(kernel_body, nz, ny), out_shape=(pltpu.V...  65 us
    unnamed x2, local copies, waits for them, and re-layouts  1.36 us

profile of v5, /device:TPU:1, one launch (start us, length us, event | category | flops | bytes accessed | tf_op | source)
XLA Modules:
  0.0 67.0 jit_solution(12843422493852892013)
XLA Ops:
  0.6 65.0 %shard_map.158 = (bf16[128,2048]{1,0:T(8,128)(2,1)S(1)}, f32[2,128]{1,0:T(2,128)S(1)}) custom-call(bf16[128,2048]{1,0:T(8,128)(2,1)} %tok_hbm.1, f32[1,2048]{1,0:T(1,128)} %bitcast.16, bf16[64,2048]{1,0:T(8,128)(2,1)} %bitcast.10, bf16[64,2048]{1,0:T(8,128)(2,1)} %bitcast.11, bf16[64,2048]{1,0:T(8,128)(2,1)} %bitcast.12, bf16[64,2048]{1,0:T(8,128)(2,1)} %bitcast.13, ...), custom_call_target="tpu_custom_call" | custom-call | tf_op jit(solution)/shard_map/pallas_call | solution.py:711
  65.6 0.8 %copy.19 = bf16[128,2048]{1,0:T(8,128)(2,1)} copy(bf16[128,2048]{1,0:T(8,128)(2,1)S(1)} %get-tuple-element.2) | data formatting | bytes 1048576
  66.4 0.6 copy.20

commit v6 on v5

--- a/solution.py
+++ b/solution.py
@@ -614,6 +614,19 @@
         lws_ref[head:head + 1, :] = top[:, :ROWS] + jnp.log(total[:, :ROWS])
         return (att.T * attg_ref[...] * 0.8).astype(BF16)
 
+    def own_merged(head, dist, value):
+        _, me, size, dev = rings[head]
+        for side in (1, 0):
+            if dist <= reach(side, size):
+                value = combine(value, await_partial(head, side, dist, dev, me))
+        return value
+
+    phase("merge_near")
+    for head, _, size, _ in rings:
+        top, total, num = own_merged(head, 1, load_own(head, 0, size))
+        stat[head, 2:3, :2 * ROWS] = top
+        stat[head, 3:4, :2 * ROWS] = total
+        acc[head, :, :2 * ROWS] = num
     phase("rec_result")
     all_of(in_r, ny - 1, in_send.at[0], in_recv.at[0]).wait_recv()
     rec = []
@@ -629,12 +642,8 @@
         half_out[k] = dot_nn(rec_rows, wo[1, :, k * width:(k + 1) * width])
 
     phase("merge_own")
-    values = [load_own(head, 0, size) for head, _, size, _ in rings]
-    for dist in (1, 2):
-        for head, me, size, dev in rings:
-            for side in (1, 0):
-                if dist <= reach(side, size):
-                    values[head] = combine(values[head], await_partial(head, side, dist, dev, me))
+    values = [own_merged(head, 2, (stat[head, 2:3, :2 * ROWS], stat[head, 3:4, :2 * ROWS], acc[head, :, :2 * ROWS]))
+              for head in (0, 1)]
     att = [finish(head, values[head]) for head in (0, 1)]
     att_rows = jnp.concatenate(att, axis=1)
 

time: 67.1 us -> 67.1 us (level)
  no operation moved by 1% of the time
where the time goes in v6:
time: 67.1 us; the launch traced here: 67 us
  Pallas kernels  65 us (97%)
  local copies, waits for them, and re-layouts  1.36 us (2%)
    pallas_call x1, Pallas kernels, on_device(): pl.pallas_call(functools.partial(kernel_body, nz, ny), out_shape=(pltpu.V...  65 us
    unnamed x2, local copies, waits for them, and re-layouts  1.36 us

profile of v6, /device:TPU:1, one launch (start us, length us, event | category | flops | bytes accessed | tf_op | source)
XLA Modules:
  0.0 67.0 jit_solution(4344682121349647091)
XLA Ops:
  0.6 65.0 %shard_map.158 = (bf16[128,2048]{1,0:T(8,128)(2,1)S(1)}, f32[2,128]{1,0:T(2,128)S(1)}) custom-call(bf16[128,2048]{1,0:T(8,128)(2,1)} %tok_hbm.1, f32[1,2048]{1,0:T(1,128)} %bitcast.16, bf16[64,2048]{1,0:T(8,128)(2,1)} %bitcast.10, bf16[64,2048]{1,0:T(8,128)(2,1)} %bitcast.11, bf16[64,2048]{1,0:T(8,128)(2,1)} %bitcast.12, bf16[64,2048]{1,0:T(8,128)(2,1)} %bitcast.13, ...), custom_call_target="tpu_custom_call" | custom-call | tf_op jit(solution)/shard_map/pallas_call | solution.py:720
  65.6 0.8 %copy.19 = bf16[128,2048]{1,0:T(8,128)(2,1)} copy(bf16[128,2048]{1,0:T(8,128)(2,1)S(1)} %get-tuple-element.2) | data formatting | bytes 1048576
  66.4 0.6 copy.20
